TPU v7x, 32 devices: a whole 2x2x4 slice. The times are simulated.
32 devices in a mesh: sp: 2 (over x), tp: 16 (over z, y, core).
Axes of the slice: x: 2, y: 2, z: 4, core: 2. Of those that a mesh axis runs over, the one named last changes fastest.
Arguments:
- query_first: bfloat16 [1024, 1536], P('sp', 'tp'), may hold values from -10 to 10
- query_second: bfloat16 [1024, 2560], P('sp', 'tp'), may hold values from -10 to 10
- latent: bfloat16 [1024, 512], P('sp'), may hold values from -400 to 400
- key_rotary: bfloat16 [1024, 32], P('sp'), may hold values from -90 to 90
- latent_gain: float32 [512], replicated, may hold values from 0.1 to 1.9
- key_up_first: bfloat16 [512, 1024], P(None, 'tp'), may hold values from -0.25 to 0.25
- value_up_first: bfloat16 [512, 1024], P(None, 'tp'), may hold values from -0.25 to 0.25
- key_up_second: bfloat16 [512, 2048], P(None, 'tp'), may hold values from -0.25 to 0.25
- value_up_second: bfloat16 [512, 2048], P(None, 'tp'), may hold values from -0.25 to 0.25
- out_first: bfloat16 [1024, 2048], P('tp'), may hold values from -0.109375 to 0.109375
- out_second: bfloat16 [2048, 2048], P('tp'), may hold values from -0.109375 to 0.109375
- residual: bfloat16 [1024, 2048], P('sp'), may hold values from -16 to 16
- expert_gain: float32 [2048], replicated, may hold values from 0.1 to 1.9
- route_experts: int32 [1024, 2], P('sp'), may hold values from 0 to 31, all different within a row; in each aligned block of 32 rows (0 to 31, 32 to 63, ...) at most 3 rows name the same one
- route_scores: float32 [1024, 2], P('sp'), may hold values from -6 to 306
- gate_weight: bfloat16 [32, 2048, 4096], P('sp', None, 'tp'), may hold values from -0.375 to 0.375
- up_weight: bfloat16 [32, 2048, 4096], P('sp', None, 'tp'), may hold values from -0.375 to 0.375
- down_weight: bfloat16 [32, 4096, 2048], P('sp', 'tp'), may hold values from -0.013671875 to 0.013671875
Outputs:
- mixed: bfloat16 [1024, 2048], P(('sp', 'tp'))
Inputs may be any that keep to these rules, and one draw needn't show every extreme that they name: `route_experts`: each row names 2 different experts. In every aligned block of 32 rows no expert is named more than 3 times, and in some blocks one is named exactly 3 times.
All inputs are finite; a program needn't handle non-finite values.
Results may differ from a plain program's by a relative error of at most 0.02.
The roundings to bfloat16 on the way count: a program that leaves them out, or rounds other values in their place, can miss the bound.
Values may be sent and summed in bfloat16 or wider, within the bound.
A program may use at most 128 MiB of HBM per device.

v0:
```python
import functools

import jax
import jax.numpy as jnp
from jax import lax
from jax.experimental import pallas as pl
from jax.experimental.pallas import tpu as pltpu
from jax.sharding import PartitionSpec as P

NA = 64
NB = 128
ROPE = 32
CAP = 3


norm_epsilon = 1e-06
rotary_base = 10000.0
clamp_limit = 7.0
sigmoid_slope = 1.702
masked_score = -1e30


def rotate(values, positions):
    half = values.shape[-1] // 2
    inverse = rotary_base ** (-jnp.arange(half, dtype=jnp.float32) / half)
    angles = positions.astype(jnp.float32)[:, None, None] * inverse[None, None, :]
    cosine = jnp.cos(angles)
    sine = jnp.sin(angles)
    first = values[..., :half]
    second = values[..., half:]
    return jnp.concatenate(
        [first * cosine - second * sine, second * cosine + first * sine], axis=-1
    )


def rms_scaled(values, gain):
    wide = values.astype(jnp.float32)
    return wide * lax.rsqrt(jnp.mean(wide * wide, axis=-1, keepdims=True) + norm_epsilon) * gain


def turned_queries(query, nope, positions):
    shaped = query.reshape(query.shape[0], query.shape[1] // (nope + ROPE), nope + ROPE)
    turned = rotate(shaped[..., nope:].astype(jnp.float32), positions).astype(jnp.bfloat16)
    return jnp.concatenate([shaped[..., :nope], turned], axis=-1)


def clamped_unit(gate, upward):
    limited = jnp.minimum(gate, clamp_limit)
    bounded = jnp.clip(upward, -clamp_limit, clamp_limit)
    return (bounded + 1.0) * limited * jax.nn.sigmoid(sigmoid_slope * limited)


def slot_numbers(chosen, experts):
    hits = (chosen[..., None] == jnp.arange(experts, dtype=jnp.int32)).astype(jnp.int32)
    before = jnp.cumsum(hits, axis=-2) - hits
    return chosen * CAP + jnp.sum(before * hits, axis=-1)


def fold_group(state, queries, key_nope, key_turned, values, query_places, scale):
    running, denominator, numerator = state
    heads = queries.shape[1]
    nope = queries.shape[2] - key_turned.shape[1]
    keys = key_nope.reshape(key_nope.shape[0], heads, nope)
    value_rows = values.reshape(values.shape[0], heads, values.shape[1] // heads)
    score = jnp.einsum(
        "qhd,khd->qhk", queries[..., :nope], keys, preferred_element_type=jnp.float32
    )
    score = score + jnp.einsum(
        "qhr,kr->qhk", queries[..., nope:], key_turned, preferred_element_type=jnp.float32
    )
    score = score * scale
    key_places = jnp.arange(keys.shape[0], dtype=jnp.int32)
    allowed = (query_places[:, None] >= key_places[None, :])[:, None, :]
    score = jnp.where(allowed, score, masked_score)
    highest = jnp.maximum(running, jnp.max(score, axis=-1))
    weights = jnp.where(allowed, jnp.exp(score - highest[..., None]), 0.0)
    denominator = jnp.sum(weights, axis=-1)
    numerator = jnp.einsum(
        "qhk,khd->qhd", weights.astype(jnp.bfloat16), value_rows, preferred_element_type=jnp.float32
    )
    return (highest, denominator, numerator)


def expert_hidden(rows, gate_weight, up_weight):
    gate = jnp.einsum("nsecd,edf->nsecf", rows, gate_weight, preferred_element_type=jnp.float32)
    upward = jnp.einsum("nsecd,edf->nsecf", rows, up_weight, preferred_element_type=jnp.float32)
    return clamped_unit(gate, upward).astype(jnp.bfloat16)


def slot_body(
    query_first,
    query_second,
    latent,
    key_rotary,
    latent_gain,
    key_up_first,
    value_up_first,
    key_up_second,
    value_up_second,
    out_first,
    out_second,
    residual,
    expert_gain,
    route_experts,
    route_scores,
    gate_weight,
    up_weight,
    down_weight,
):
    seq_rows = latent.shape[0]
    sets = lax.axis_size("tp")
    groups = lax.axis_size("sp")
    own_rows = seq_rows // sets
    topk = route_experts.shape[1]
    local_experts = gate_weight.shape[0]
    experts = local_experts * groups
    offset = lax.axis_index("sp") * seq_rows
    places = offset + jnp.arange(seq_rows, dtype=jnp.int32)
    last_place = offset + seq_rows - 1
    queries_first = turned_queries(query_first, NA, places)
    queries_second = turned_queries(query_second, NB, places)
    key_turned = rotate(key_rotary.astype(jnp.float32)[:, None, :], places)[:, 0, :].astype(
        jnp.bfloat16
    )
    latent_normed = rms_scaled(latent, latent_gain).astype(jnp.bfloat16)
    scale_first = (NA + ROPE) ** (-0.5)
    scale_second = (NB + ROPE) ** (-0.5)

    def attend(carry, parts):
        key_first, value_first, key_second, value_second, turned = parts
        return (
            fold_group(
                carry[0], queries_first, key_first, turned, value_first, places, scale_first
            ),
            fold_group(
                carry[1], queries_second, key_second, turned, value_second, places, scale_second
            ),
        )

    def initial(queries, value_width):
        shape = queries.shape[:2]
        return (
            jnp.full(shape, masked_score, jnp.float32),
            jnp.zeros(shape, jnp.float32),
            jnp.zeros(shape + (value_width,), jnp.float32),
        )

    start_state = (
        initial(queries_first, value_up_first.shape[1] // queries_first.shape[1]),
        initial(queries_second, value_up_second.shape[1] // queries_second.shape[1]),
    )
    key_first, value_first, key_second, value_second = tuple(
        (
            jnp.dot(latent_normed, weight, preferred_element_type=jnp.float32).astype(jnp.bfloat16)
            for weight in (key_up_first, value_up_first, key_up_second, value_up_second)
        )
    )
    parts = (
        lax.all_gather(key_first, "sp", axis=0, tiled=True),
        lax.all_gather(value_first, "sp", axis=0, tiled=True),
        lax.all_gather(key_second, "sp", axis=0, tiled=True),
        lax.all_gather(value_second, "sp", axis=0, tiled=True),
        lax.all_gather(key_turned, "sp", axis=0, tiled=True),
    )
    state = lax.cond(
        jnp.int32(0) <= last_place,
        lambda inner: attend(inner, parts),
        lambda inner: inner,
        start_state,
    )
    first_state, second_state = state
    attended_first = (
        (first_state[2] / first_state[1][..., None]).astype(jnp.bfloat16).reshape(seq_rows, -1)
    )
    attended_second = (
        (second_state[2] / second_state[1][..., None]).astype(jnp.bfloat16).reshape(seq_rows, -1)
    )
    own_start = lax.axis_index("tp") * own_rows
    slot_range = jnp.arange(experts * CAP, dtype=jnp.int32)
    projected = lax.psum_scatter(
        (
            jnp.dot(attended_first, out_first, preferred_element_type=jnp.float32)
            + jnp.dot(attended_second, out_second, preferred_element_type=jnp.float32)
        ).astype(jnp.bfloat16),
        "tp",
        scatter_dimension=0,
        tiled=True,
    ).astype(jnp.float32)
    own_residual = lax.dynamic_slice_in_dim(residual, own_start, own_rows, 0)
    middle = (own_residual.astype(jnp.float32) + projected).astype(jnp.bfloat16)
    normed = rms_scaled(middle, expert_gain).astype(jnp.bfloat16)
    own_ids = lax.dynamic_slice_in_dim(route_experts, own_start, own_rows, 0).reshape(-1)
    own_slots = slot_numbers(own_ids, experts)
    picks = (own_slots[:, None] == slot_range).reshape(own_rows, topk, experts * CAP)
    selected = jnp.sum(picks.astype(jnp.float32), axis=1).astype(jnp.bfloat16)
    outgoing = jnp.einsum("ts,td->sd", selected, normed, preferred_element_type=jnp.float32).astype(
        jnp.bfloat16
    )
    outgoing = outgoing.reshape(groups, local_experts, CAP, outgoing.shape[-1])
    arrived = lax.all_to_all(outgoing, "sp", split_axis=0, concat_axis=0, tiled=True)
    activated = expert_hidden(
        lax.all_gather(arrived[None], "tp", axis=0, tiled=True), gate_weight, up_weight
    )
    flat_hidden = activated.reshape(sets * groups, local_experts, CAP, activated.shape[-1])
    summed = lax.psum_scatter(
        jnp.einsum(
            "secf,efd->secd", flat_hidden, down_weight, preferred_element_type=jnp.float32
        ).astype(jnp.bfloat16),
        "tp",
        scatter_dimension=0,
        tiled=True,
    )
    returned = lax.all_to_all(summed, "sp", split_axis=0, concat_axis=0, tiled=True)
    expert_out = returned.reshape(experts * CAP, returned.shape[-1]).astype(jnp.float32)
    own_scores = lax.dynamic_slice_in_dim(route_scores, own_start, own_rows, 0)
    route_weight = jax.nn.softmax(own_scores, axis=-1)
    matches = own_slots.reshape(own_rows, topk)[..., None] == slot_range
    combine = jnp.sum(jnp.where(matches, route_weight[..., None], 0.0), axis=1)
    mixture = jnp.dot(combine, expert_out, precision=lax.Precision.HIGHEST)
    return (middle.astype(jnp.float32) + mixture).astype(jnp.bfloat16)


MESH = pl.DeviceIdType.MESH
VMEM = pl.BlockSpec(memory_space=pltpu.VMEM)
TILE_TOKENS = 256


def places_of(axes):
    return {axis: lax.axis_index(axis) for axis in axes}


def bit_of(place, step):
    axis, mask = step
    return (place[axis] // mask) % 2


def partner_of(place, step):
    axis, mask = step
    return {axis: place[axis] + mask * (1 - 2 * bit_of(place, step))}


def greet(place, steps):
    barrier = pltpu.get_barrier_semaphore()
    for step in steps:
        pl.semaphore_signal(
            barrier, inc=1, device_id=partner_of(place, step), device_id_type=MESH
        )
    pl.semaphore_wait(barrier, len(steps))


def cube_steps(sp, tp):
    core = [("tp", 1)] if tp > 1 else []
    first = [("tp", 2)] if tp > 2 else []
    rest = [("tp", 1 << i) for i in range(2, tp.bit_length() - 1)]
    across = [("sp", 1 << i) for i in range(sp.bit_length() - 1)]
    return core, first, rest, across


def weight_of(step, widths):
    axis, mask = step
    return mask * (widths if axis == "sp" else 1)


def base_of(place, fixed, width):
    total = jnp.int32(0)
    for step in fixed:
        total = total + bit_of(place, step) * weight_of(step, width)
    return total


def offsets_of(free, width):
    found = [0]
    for step in free:
        found = found + [one + weight_of(step, width) for one in found]
    return found


def block_rows_of(index, rows):
    return pl.ds(pl.multiple_of(index * rows, rows), rows)


def gather_kernel(orders, width, x_ref, out_ref, send_sem, recv_sem, own_sem):
    place = places_of(("sp", "tp"))
    steps = orders[0]
    rows = x_ref.shape[0]
    cols = x_ref.shape[1] // len(orders)
    greet(place, steps)
    own = pltpu.make_async_copy(
        x_ref, out_ref.at[block_rows_of(base_of(place, steps, width), rows), :], own_sem
    )
    own.start()

    def columns(part):
        return pl.ds(part * cols, cols)

    def start(part, number):
        order = orders[part]
        base = base_of(place, order[number:], width)
        for offset in offsets_of(order[:number], width):
            spot = out_ref.at[block_rows_of(base + offset, rows), columns(part)]
            source = x_ref.at[:, columns(part)] if number == 0 else spot
            pltpu.make_async_remote_copy(
                src_ref=source,
                dst_ref=spot,
                send_sem=send_sem.at[part, number],
                recv_sem=recv_sem.at[part, number],
                device_id=partner_of(place, order[number]),
                device_id_type=MESH,
            ).start()

    def drain(part, number, sem):
        whole = out_ref.at[pl.ds(0, rows << number), columns(part)]
        pltpu.make_async_copy(whole, whole, sem.at[part, number]).wait()

    for part in range(len(orders)):
        start(part, 0)
    own.wait()
    for wave in range(len(steps) + 1):
        for part in range(len(orders)):
            number = wave - part // 2 % 2
            if number < 0 or number >= len(steps):
                continue
            drain(part, number, recv_sem)
            if number + 1 < len(steps):
                start(part, number + 1)
    for part in range(len(orders)):
        for number in range(len(steps)):
            drain(part, number, send_sem)


def gather_blocks(x, orders, width, count, collective_id):
    rows, depth = x.shape
    parts, stages = len(orders), len(orders[0])
    return pl.pallas_call(
        functools.partial(gather_kernel, orders, width),
        out_shape=jax.ShapeDtypeStruct((rows * count, depth), x.dtype),
        in_specs=[VMEM],
        out_specs=VMEM,
        scratch_shapes=[
            pltpu.SemaphoreType.DMA((parts, stages)),
            pltpu.SemaphoreType.DMA((parts, stages)),
            pltpu.SemaphoreType.DMA,
        ],
        compiler_params=pltpu.CompilerParams(
            collective_id=collective_id, has_side_effects=True, vmem_limit_bytes=8 << 20
        ),
        name="gather_blocks",
    )(x)


def scatter_kernel(
    orders, width, rows, x_ref, out_ref, total_ref, landing_ref, send_sem, recv_sem
):
    place = places_of(("sp", "tp"))
    stages = len(orders[0])
    cols = x_ref.shape[1] // len(orders)
    greet(place, orders[0])
    spots = [0]
    for number in range(stages):
        spots.append(spots[-1] + (1 << (stages - 1 - number)))

    def columns(part):
        return pl.ds(part * cols, cols)

    def start(part, number):
        order = orders[part]
        step = order[number]
        source = x_ref if number == 0 else total_ref
        base = base_of(place, order[:number], width)
        base = base + (1 - bit_of(place, step)) * weight_of(step, width)
        for slot, offset in enumerate(offsets_of(order[number + 1 :], width)):
            pltpu.make_async_remote_copy(
                src_ref=source.at[block_rows_of(base + offset, rows), columns(part)],
                dst_ref=landing_ref.at[pl.ds((spots[number] + slot) * rows, rows), columns(part)],
                send_sem=send_sem.at[part, number],
                recv_sem=recv_sem.at[part, number],
                device_id=partner_of(place, step),
                device_id_type=MESH,
            ).start()

    def drain(part, number, sem):
        count = 1 << (stages - 1 - number)
        whole = landing_ref.at[pl.ds(spots[number] * rows, count * rows), columns(part)]
        pltpu.make_async_copy(whole, whole, sem.at[part, number]).wait()

    def add(part, number):
        order = orders[part]
        source = x_ref if number == 0 else total_ref
        base = base_of(place, order[: number + 1], width)
        for slot, offset in enumerate(offsets_of(order[number + 1 :], width)):
            here = block_rows_of(base + offset, rows)
            there = pl.ds((spots[number] + slot) * rows, rows)
            value = source[here, columns(part)].astype(jnp.float32) + landing_ref[
                there, columns(part)
            ].astype(jnp.float32)
            if number + 1 < stages:
                total_ref[here, columns(part)] = value.astype(total_ref.dtype)
            else:
                out_ref[:, columns(part)] = value

    for part in range(len(orders)):
        start(part, 0)
    for wave in range(stages + 1):
        for part in range(len(orders)):
            number = wave - part // 2 % 2
            if number < 0 or number >= stages:
                continue
            drain(part, number, recv_sem)
            add(part, number)
            if number + 1 < stages:
                start(part, number + 1)
    for part in range(len(orders)):
        for number in range(stages):
            drain(part, number, send_sem)


def scatter_blocks(x, orders, width, count, collective_id):
    rows = x.shape[0] // count
    depth = x.shape[1]
    parts, stages = len(orders), len(orders[0])
    return pl.pallas_call(
        functools.partial(scatter_kernel, orders, width, rows),
        out_shape=jax.ShapeDtypeStruct((rows, depth), jnp.float32),
        in_specs=[VMEM],
        out_specs=VMEM,
        scratch_shapes=[
            pltpu.VMEM(x.shape, x.dtype),
            pltpu.VMEM(((count - 1) * rows, depth), x.dtype),
            pltpu.SemaphoreType.DMA((parts, stages)),
            pltpu.SemaphoreType.DMA((parts, stages)),
        ],
        compiler_params=pltpu.CompilerParams(
            collective_id=collective_id, has_side_effects=True, vmem_limit_bytes=16 << 20
        ),
        name="scatter_blocks",
    )(x)


def exchange_kernel(latent_ref, turn_ref, route_ref, l_out, t_out, r_out, send_sem, recv_sem, own_sem):
    place = places_of(("sp", "tp"))
    across, core = ("sp", 1), ("tp", 1)
    greet(place, (across, core))
    half = latent_ref.shape[0] // 2
    side = bit_of(place, core)
    me = place["sp"]
    other = 1 - me
    pairs = ((latent_ref, l_out), (turn_ref, t_out))
    mine = pl.ds(pl.multiple_of(side * half, half), half)
    crossing = []
    for number, (source, target) in enumerate(pairs):
        crossing.append(
            pltpu.make_async_remote_copy(
                src_ref=source.at[mine, :],
                dst_ref=target.at[me, mine, :],
                send_sem=send_sem.at[number],
                recv_sem=recv_sem.at[number],
                device_id=partner_of(place, across),
                device_id_type=MESH,
            )
        )
    crossing.append(
        pltpu.make_async_remote_copy(
            src_ref=route_ref,
            dst_ref=r_out.at[me],
            send_sem=send_sem.at[2],
            recv_sem=recv_sem.at[2],
            device_id=partner_of(place, across),
            device_id_type=MESH,
        )
    )
    for copy in crossing:
        copy.start()
    kept = [
        pltpu.make_async_copy(source, target.at[me], own_sem.at[number])
        for number, (source, target) in enumerate(pairs + ((route_ref, r_out),))
    ]
    for copy in kept:
        copy.start()
    passing = []
    for number, (source, target) in enumerate(pairs):
        crossing[number].wait_recv()
        spot = target.at[other, mine, :]
        copy = pltpu.make_async_remote_copy(
            src_ref=spot,
            dst_ref=spot,
            send_sem=send_sem.at[3 + number],
            recv_sem=recv_sem.at[3 + number],
            device_id=partner_of(place, core),
            device_id_type=MESH,
        )
        copy.start()
        passing.append(copy)
    crossing[2].wait_recv()
    for copy in crossing:
        copy.wait_send()
    for copy in kept + passing:
        copy.wait()


def exchange(latent, turn, route, collective_id):
    return pl.pallas_call(
        exchange_kernel,
        out_shape=tuple(
            jax.ShapeDtypeStruct((2,) + one.shape, one.dtype) for one in (latent, turn, route)
        ),
        in_specs=[VMEM] * 3,
        out_specs=(VMEM,) * 3,
        scratch_shapes=[
            pltpu.SemaphoreType.DMA((5,)),
            pltpu.SemaphoreType.DMA((5,)),
            pltpu.SemaphoreType.DMA((3,)),
        ],
        compiler_params=pltpu.CompilerParams(collective_id=collective_id, has_side_effects=True),
        name="exchange",
    )(latent, turn, route)


def expert_kernel(pitch, x_ref, code_ref, gate_ref, up_ref, down_ref, out_ref, rows_ref, scale_ref):
    index = pl.program_id(0)
    experts = pl.num_programs(0)
    tiles, count, _, depth = rows_ref.shape
    span = count * pitch
    tokens = x_ref.shape[0] // tiles

    def hits(tile, choice):
        wanted = code_ref[tile, pl.ds(choice, 1), :]
        slots = lax.broadcasted_iota(jnp.int32, (span, tokens), 0)
        return slots == wanted.astype(jnp.int32)

    @pl.when(index == 0)
    def _():
        for tile in range(tiles):
            first, second = hits(tile, 0), hits(tile, 1)
            chosen = jnp.where(first | second, 1.0, 0.0).astype(jnp.bfloat16)
            picked = jnp.dot(
                chosen,
                x_ref[pl.ds(tile * tokens, tokens), :],
                preferred_element_type=jnp.float32,
            ).astype(jnp.bfloat16)
            rows_ref[tile] = picked.reshape(count, pitch, depth)
            share = jnp.where(first, code_ref[tile, pl.ds(2, 1), :], 0.0) + jnp.where(
                second, code_ref[tile, pl.ds(3, 1), :], 0.0
            )
            scale_ref[tile] = jnp.sum(share, axis=1, keepdims=True).reshape(count, pitch, 1)

    rows = rows_ref[:, index].reshape(tiles * pitch, depth)
    gate = jnp.dot(rows, gate_ref[0], preferred_element_type=jnp.float32)
    upward = jnp.dot(rows, up_ref[0], preferred_element_type=jnp.float32)
    activated = clamped_unit(gate, upward).astype(jnp.bfloat16)
    result = jnp.dot(activated, down_ref[0], preferred_element_type=jnp.float32)
    scaled = result * scale_ref[:, index].reshape(tiles * pitch, 1)
    rows_ref[:, index] = scaled.astype(jnp.bfloat16).reshape(tiles, pitch, depth)

    @pl.when(index == experts - 1)
    def _():
        for tile in range(tiles):
            chosen = jnp.where(hits(tile, 0) | hits(tile, 1), 1.0, 0.0).astype(jnp.bfloat16)
            out_ref[pl.ds(tile * tokens, tokens), :] = lax.dot_general(
                chosen,
                rows_ref[tile].reshape(span, depth),
                (((0,), (0,)), ((), ())),
                preferred_element_type=jnp.float32,
            ).astype(jnp.bfloat16)


def run_experts(tokens, codes, gate_weight, up_weight, down_weight, pitch):
    experts, depth, units = gate_weight.shape
    tiles = codes.shape[0]
    return pl.pallas_call(
        functools.partial(expert_kernel, pitch),
        grid=(experts,),
        out_shape=jax.ShapeDtypeStruct(tokens.shape, jnp.bfloat16),
        in_specs=[
            pl.BlockSpec(tokens.shape, lambda i: (0, 0)),
            pl.BlockSpec(codes.shape, lambda i: (0, 0, 0)),
            pl.BlockSpec((1, depth, units), lambda i: (i, 0, 0)),
            pl.BlockSpec((1, depth, units), lambda i: (i, 0, 0)),
            pl.BlockSpec((1, units, depth), lambda i: (i, 0, 0)),
        ],
        out_specs=pl.BlockSpec(tokens.shape, lambda i: (0, 0)),
        scratch_shapes=[
            pltpu.VMEM((tiles, experts, pitch, depth), jnp.bfloat16),
            pltpu.VMEM((tiles, experts, pitch, 1), jnp.float32),
        ],
        compiler_params=pltpu.CompilerParams(
            dimension_semantics=("arbitrary",), vmem_limit_bytes=36 << 20
        ),
        name="run_experts",
    )(tokens, codes, gate_weight, up_weight, down_weight)


def attended_heads(queries, nope, keys, turned, values, allowed, scale):
    heads = queries.shape[1]
    wide = keys.reshape(keys.shape[0], heads, nope)
    shared = jnp.broadcast_to(turned[:, None, :], (turned.shape[0], heads, turned.shape[1]))
    whole = jnp.concatenate([wide, shared], axis=-1)
    value_rows = values.reshape(values.shape[0], heads, values.shape[1] // heads)
    score = jnp.einsum("qhd,khd->hqk", queries, whole, preferred_element_type=jnp.float32) * scale
    score = jnp.where(allowed, score, masked_score)
    highest = jnp.max(score, axis=-1, keepdims=True)
    weights = jnp.exp(score - highest)
    denominator = jnp.sum(weights, axis=-1)
    numerator = jnp.einsum(
        "hqk,khd->hqd", weights.astype(jnp.bfloat16), value_rows, preferred_element_type=jnp.float32
    )
    attended = (numerator / denominator[..., None]).astype(jnp.bfloat16)
    return jnp.swapaxes(attended, 0, 1).reshape(attended.shape[1], -1)


def token_body(
    query_first,
    query_second,
    latent,
    key_rotary,
    latent_gain,
    key_up_first,
    value_up_first,
    key_up_second,
    value_up_second,
    out_first,
    out_second,
    residual,
    expert_gain,
    route_experts,
    route_scores,
    gate_weight,
    up_weight,
    down_weight,
):
    seq_rows = latent.shape[0]
    sets = lax.axis_size("tp")
    groups = lax.axis_size("sp")
    own_rows = seq_rows // sets
    local_experts = gate_weight.shape[0]
    total = groups * seq_rows
    me = lax.axis_index("sp")
    core, first, rest, across = cube_steps(groups, sets)
    span_blocks = TILE_TOKENS // own_rows
    pitch = -(-span_blocks * CAP // 16) * 16

    chosen = route_experts.reshape(sets, -1)
    earlier = jnp.tril(jnp.ones((chosen.shape[1],) * 2, jnp.float32), -1)
    same = (chosen[:, :, None] == chosen[:, None, :]).astype(jnp.float32)
    rank = jnp.sum(same * earlier, axis=-1)
    spot = ((jnp.arange(sets, dtype=jnp.int32) % span_blocks) * CAP).astype(jnp.float32)
    code = chosen.astype(jnp.float32) * pitch + spot[:, None] + rank
    code = code.reshape(seq_rows, -1).T
    scores = route_scores.T
    raised = jnp.exp(scores - jnp.max(scores, axis=0, keepdims=True))
    share = raised / jnp.sum(raised, axis=0, keepdims=True)
    route = jnp.concatenate([code, share, code, share], axis=0)

    rotary = key_rotary.shape[1]
    wide_rotary = jnp.pad(key_rotary, ((0, 0), (0, -rotary % 128)))
    latents, turns, routes = exchange(latent, wide_rotary, route, 0)

    places = me * seq_rows + jnp.arange(seq_rows, dtype=jnp.int32)
    all_places = jnp.arange(total, dtype=jnp.int32)
    queries_first = turned_queries(query_first, NA, places)
    queries_second = turned_queries(query_second, NB, places)
    turned = rotate(
        turns.reshape(total, -1)[:, :rotary].astype(jnp.float32)[:, None, :], all_places
    )[:, 0, :].astype(jnp.bfloat16)
    latent_normed = rms_scaled(latents.reshape(total, -1), latent_gain).astype(jnp.bfloat16)
    key_first, value_first, key_second, value_second = tuple(
        jnp.dot(latent_normed, weight, preferred_element_type=jnp.float32).astype(jnp.bfloat16)
        for weight in (key_up_first, value_up_first, key_up_second, value_up_second)
    )
    allowed = (places[:, None] >= all_places[None, :])[None]
    attended_first = attended_heads(
        queries_first, NA, key_first, turned, value_first, allowed, (NA + ROPE) ** (-0.5)
    )
    attended_second = attended_heads(
        queries_second, NB, key_second, turned, value_second, allowed, (NB + ROPE) ** (-0.5)
    )
    partial = (
        jnp.dot(attended_first, out_first, preferred_element_type=jnp.float32)
        + jnp.dot(attended_second, out_second, preferred_element_type=jnp.float32)
    ).astype(jnp.bfloat16)
    one, two = tuple(core + first + rest), tuple(core + rest + first)
    projected = scatter_blocks(partial, (one, two, one, one), sets, sets, 1)
    own_start = lax.axis_index("tp") * own_rows
    own_residual = lax.dynamic_slice_in_dim(residual, own_start, own_rows, 0)
    middle = (own_residual.astype(jnp.float32) + projected).astype(jnp.bfloat16)
    normed = rms_scaled(middle, expert_gain).astype(jnp.bfloat16)
    ladder = rest[::-1]
    one = tuple(ladder + across + first + core)
    two = tuple(ladder + first + across + core)
    tokens = gather_blocks(normed, (one, two, one, two), sets, groups * sets, 2)

    tiles = total // TILE_TOKENS
    codes = jnp.swapaxes(routes, 0, 1).reshape(8, total)
    shift = jnp.array([1.0, 1.0, 0.0, 0.0, 1.0, 1.0, 0.0, 0.0], jnp.float32)
    codes = codes - (shift * (me * local_experts * pitch).astype(jnp.float32))[:, None]
    codes = jnp.swapaxes(codes.reshape(8, tiles, TILE_TOKENS), 0, 1)
    mixed = run_experts(tokens, codes, gate_weight, up_weight, down_weight, pitch)
    one, two = one[::-1], two[::-1]
    mixture = scatter_blocks(mixed, (one, two, one, two), sets, groups * sets, 3)
    return (middle.astype(jnp.float32) + mixture).astype(jnp.bfloat16)


def solution(mesh):
    in_specs = (
        P("sp", "tp"),
        P("sp", "tp"),
        P("sp", None),
        P("sp", None),
        P(),
        P(None, "tp"),
        P(None, "tp"),
        P(None, "tp"),
        P(None, "tp"),
        P("tp", None),
        P("tp", None),
        P("sp", None),
        P(),
        P("sp", None),
        P("sp", None),
        P("sp", None, "tp"),
        P("sp", None, "tp"),
        P("sp", "tp", None),
    )
    out_specs = P(("sp", "tp"), None)
    groups, sets = mesh.shape["sp"], mesh.shape["tp"]
    small = groups == 2 and sets & (sets - 1) == 0 and sets > 2

    def body(*arguments):
        fits = small and arguments[2].shape[0] * groups <= 1024
        return (token_body if fits else slot_body)(*arguments)

    return jax.shard_map(body, mesh=mesh, in_specs=in_specs, out_specs=out_specs, check_vma=False)
```

profile of v0, /device:TPU:0, one launch (start us, length us, event | category | flops | bytes accessed | tf_op | source)
XLA Modules:
  0.0 164.9 jit_solution(12486955647273804713)
XLA Ops:
  0.0 0.7 broadcast_multiply_fusion
  0.7 0.7 reduce_max.27
  1.5 0.7 fusion.61
  2.4 0.9 slice.44
  3.3 0.9 slice.51
  4.2 0.9 copy.26
  5.1 0.7 pad.4.turn_ref
  5.8 0.8 slice_convert_fusion
  6.8 0.8 copy.27
  9.2 14.8 %exchange.1 = (bf16[2,512,512]{2,1,0:T(8,128)(2,1)}, bf16[2,512,128]{2,1,0:T(8,128)(2,1)}, f32[2,8,512]{2,1,0:T(8,128)}) custom-call(bf16[512,512]{1,0:T(8,128)(2,1)} %latent_ref.1, bf16[512,128]{1,0:T(8,128)(2,1)} %pad.4.turn_ref, f32[8,512]{1,0:T(8,128)} %pad_maximum_fusion.route_ref), custom_call_target="tpu_custom_call" | custom-call | tf_op jit(solution)/shard_map/exchange/pallas_call | solution.py:501
  24.0 1.1 copy.30
  25.1 0.8 subtract_bitcast_fusion.code_ref
  26.0 1.5 multiply_reduce_fusion
  29.8 1.3 copy-done.4
  31.7 2.7 %fusion.9 = bf16[512,128]{1,0:T(8,128)(2,1)S(1)} fusion(bf16[1024,512]{1,0:T(8,128)(2,1)S(1)} %fusion.1, bf16[512,128]{1,0:T(8,128)(2,1)S(1)} %copy-done.13, f32[512,1024]{1,0:T(8,128)} %copy-done.4, f32[512]{0:T(512)S(1)} %get-tuple-element.21, f32[512]{0:T(512)S(1)} %fusion.4), kind=kOutput, calls=%fused_computation.19 | convolution fusion | flops 269746176 | bytes 3411968 | tf_op jit(solution)/shard_map/hqk,khd->hqd/dot_general | solution.py:603
  35.1 1.4 copy-done.2
  36.9 2.4 %fusion.11 = bf16[512,64]{0,1:T(8,128)(2,1)S(1)} fusion(bf16[1024,512]{1,0:T(8,128)(2,1)S(1)} %fusion.1, bf16[512,64]{0,1:T(8,128)(2,1)S(1)} %copy-done.8, f32[512,1024]{1,0:T(8,128)} %copy-done.2, f32[512]{0:T(512)S(1)} %get-tuple-element.23, f32[512]{0:T(512)S(1)} %fusion.2), kind=kOutput, calls=%fused_computation.24 | convolution fusion | flops 135397376 | bytes 3280896 | tf_op jit(solution)/shard_map/hqk,khd->hqd/dot_general | solution.py:603
  39.3 0.7 fusion.69
  40.2 0.7 add_convert_fusion.x_ref
  41.0 25.1 %scatter_blocks.2 = f32[32,2048]{1,0:T(8,128)S(1)} custom-call(bf16[512,2048]{1,0:T(8,128)(2,1)S(1)} %add_convert_fusion.x_ref), custom_call_target="tpu_custom_call" | custom-call | tf_op jit(solution)/shard_map/scatter_blocks/pallas_call | solution.py:421
  66.1 1.1 fusion.20
  67.3 32.8 %gather_blocks.1.x_ref = bf16[1024,2048]{1,0:T(8,128)(2,1)S(1)} custom-call(bf16[32,2048]{1,0:T(8,128)(2,1)S(1)} %fusion.22.x_ref), custom_call_target="tpu_custom_call" | custom-call | tf_op jit(solution)/shard_map/gather_blocks/pallas_call | solution.py:334
  100.1 28.1 %run_experts.1.x_ref = bf16[1024,2048]{1,0:T(8,128)(2,1)S(1)} custom-call(bf16[1024,2048]{1,0:T(8,128)(2,1)S(1)} %gather_blocks.1.x_ref, f32[4,8,256]{2,1,0:T(8,128)S(1)} %subtract_bitcast_fusion.code_ref, bf16[16,2048,256]{2,1,0:T(8,128)(2,1)} %gate_ref.1, bf16[16,2048,256]{2,1,0:T(8,128)(2,1)} %up_ref.1, bf16[16,256,2048]{2,1,0:T(8,128)(2,1)} %down_ref.1), custom_call_target="tpu_custom_call" | custom-call | tf_op jit(solution)/shard_map/run_experts/pallas_call | solution.py:569
  128.2 36.1 %scatter_blocks.3 = f32[32,2048]{1,0:T(8,128)S(1)} custom-call(bf16[1024,2048]{1,0:T(8,128)(2,1)S(1)} %run_experts.1.x_ref), custom_call_target="tpu_custom_call" | custom-call | tf_op jit(solution)/shard_map/scatter_blocks/pallas_call | solution.py:421
  (55 shorter events, 7.0 us)
Async XLA Ops:
  0.0 39.3 %copy-start = (bf16[128,2048]{1,0:T(8,128)(2,1)S(1)}, bf16[128,2048]{1,0:T(8,128)(2,1)}, u32[]{:S(2)}) copy-start(bf16[128,2048]{1,0:T(8,128)(2,1)} %param.29) | copy-start | bytes 1572868
  0.0 8.5 %copy-start.9 = (f32[512,2]{0,1:T(2,128)S(1)}, f32[512,2]{0,1:T(2,128)}, u32[]{:S(2)}) copy-start(f32[512,2]{0,1:T(2,128)} %param.33) | copy-start | bytes 12292
  0.0 8.5 %copy-start.10 = (s32[512,2]{0,1:T(2,128)S(1)}, s32[512,2]{0,1:T(2,128)}, u32[]{:S(2)}) copy-start(s32[512,2]{0,1:T(2,128)} %param.32) | copy-start | bytes 12292
  4.2 23.3 %copy-start.12 = (f32[512]{0:T(512)S(1)}, f32[512]{0:T(512)}, u32[]{:S(2)}) copy-start(f32[512]{0:T(512)} %param.23) | copy-start | bytes 6148
  24.0 3.6 %copy-start.3 = (bf16[2,512,512]{2,1,0:T(8,128)(2,1)S(1)}, bf16[2,512,512]{2,1,0:T(8,128)(2,1)}, u32[]{:S(2)}) copy-start(bf16[2,512,512]{2,1,0:T(8,128)(2,1)} %get-tuple-element.8) | copy-start | bytes 3145732
  24.0 4.2 %copy-start.7 = (bf16[512,64]{0,1:T(8,128)(2,1)S(1)}, bf16[512,64]{0,1:T(8,128)(2,1)}, u32[]{:S(2)}) copy-start(bf16[512,64]{0,1:T(8,128)(2,1)} %param.24) | copy-start | bytes 196612
  27.5 1.2 copy-start.6
  29.8 1.4 copy-start.4
  29.8 1.9 %copy-start.13 = (bf16[512,128]{1,0:T(8,128)(2,1)S(1)}, bf16[512,128]{1,0:T(8,128)(2,1)}, u32[]{:S(2)}) copy-start(bf16[512,128]{1,0:T(8,128)(2,1)} %param.27) | copy-start | bytes 393220
  34.4 2.5 %copy-start.8 = (bf16[512,64]{0,1:T(8,128)(2,1)S(1)}, bf16[512,64]{0,1:T(8,128)(2,1)}, u32[]{:S(2)}) copy-start(bf16[512,64]{0,1:T(8,128)(2,1)} %param.25) | copy-start | bytes 196612
  35.0 1.4 copy-start.2
  39.3 1.0 copy-start.5
  41.0 26.2 %copy-start.11 = (f32[2048]{0:T(1024)S(1)}, f32[2048]{0:T(1024)}, u32[]{:S(2)}) copy-start(f32[2048]{0:T(1024)} %param.31) | copy-start | bytes 24580
  100.1 64.8 %copy-start.1 = (bf16[128,2048]{1,0:T(8,128)(2,1)S(1)}, bf16[128,2048]{1,0:T(8,128)(2,1)}, u32[]{:S(2)}) copy-start(bf16[128,2048]{1,0:T(8,128)(2,1)} %param.29) | copy-start | bytes 1572868
where the time goes:
time: 166 us; the launch traced here: 165 us
  Pallas kernels  137 us (83%)
  other arithmetic  10.1 us (6%)
  local copies, waits for them, and re-layouts  9 us (5%)
  matrix products  8.71 us (5%)
    pallas_call x2, Pallas kernels, scatter_blocks(): pl.pallas_call(functools.partial(scatter_kernel, orders, width, rows), ou...  61.2 us
    pallas_call x1, Pallas kernels, gather_blocks(): pl.pallas_call(functools.partial(gather_kernel, orders, width), out_shape...  32.8 us
    pallas_call x1, Pallas kernels, run_experts(): pl.pallas_call(functools.partial(expert_kernel, pitch), grid=(experts,),...  28.1 us
    pallas_call x1, Pallas kernels, exchange(): pl.pallas_call(exchange_kernel, out_shape=tuple((jax.ShapeDtypeStruct((2,...  14.8 us
    unnamed x32, local copies, waits for them, and re-layouts  5.86 us
    dot_general x2, matrix products, attended_heads(): jnp.einsum('hqk,khd->hqd', weights.astype(jnp.bfloat16), value_rows, pref...  5.09 us

commit v1 on v0

--- a/solution.py
+++ b/solution.py
@@ -223,6 +223,7 @@
 MESH = pl.DeviceIdType.MESH
 VMEM = pl.BlockSpec(memory_space=pltpu.VMEM)
 TILE_TOKENS = 256
+CHUNKS = 4
 
 
 def places_of(axes):
@@ -277,75 +278,6 @@
 
 def block_rows_of(index, rows):
     return pl.ds(pl.multiple_of(index * rows, rows), rows)
-
-
-def gather_kernel(orders, width, x_ref, out_ref, send_sem, recv_sem, own_sem):
-    place = places_of(("sp", "tp"))
-    steps = orders[0]
-    rows = x_ref.shape[0]
-    cols = x_ref.shape[1] // len(orders)
-    greet(place, steps)
-    own = pltpu.make_async_copy(
-        x_ref, out_ref.at[block_rows_of(base_of(place, steps, width), rows), :], own_sem
-    )
-    own.start()
-
-    def columns(part):
-        return pl.ds(part * cols, cols)
-
-    def start(part, number):
-        order = orders[part]
-        base = base_of(place, order[number:], width)
-        for offset in offsets_of(order[:number], width):
-            spot = out_ref.at[block_rows_of(base + offset, rows), columns(part)]
-            source = x_ref.at[:, columns(part)] if number == 0 else spot
-            pltpu.make_async_remote_copy(
-                src_ref=source,
-                dst_ref=spot,
-                send_sem=send_sem.at[part, number],
-                recv_sem=recv_sem.at[part, number],
-                device_id=partner_of(place, order[number]),
-                device_id_type=MESH,
-            ).start()
-
-    def drain(part, number, sem):
-        whole = out_ref.at[pl.ds(0, rows << number), columns(part)]
-        pltpu.make_async_copy(whole, whole, sem.at[part, number]).wait()
-
-    for part in range(len(orders)):
-        start(part, 0)
-    own.wait()
-    for wave in range(len(steps) + 1):
-        for part in range(len(orders)):
-            number = wave - part // 2 % 2
-            if number < 0 or number >= len(steps):
-                continue
-            drain(part, number, recv_sem)
-            if number + 1 < len(steps):
-                start(part, number + 1)
-    for part in range(len(orders)):
-        for number in range(len(steps)):
-            drain(part, number, send_sem)
-
-
-def gather_blocks(x, orders, width, count, collective_id):
-    rows, depth = x.shape
-    parts, stages = len(orders), len(orders[0])
-    return pl.pallas_call(
-        functools.partial(gather_kernel, orders, width),
-        out_shape=jax.ShapeDtypeStruct((rows * count, depth), x.dtype),
-        in_specs=[VMEM],
-        out_specs=VMEM,
-        scratch_shapes=[
-            pltpu.SemaphoreType.DMA((parts, stages)),
-            pltpu.SemaphoreType.DMA((parts, stages)),
-            pltpu.SemaphoreType.DMA,
-        ],
-        compiler_params=pltpu.CompilerParams(
-            collective_id=collective_id, has_side_effects=True, vmem_limit_bytes=8 << 20
-        ),
-        name="gather_blocks",
-    )(x)
 
 
 def scatter_kernel(
@@ -515,78 +447,417 @@
     )(latent, turn, route)
 
 
-def expert_kernel(pitch, x_ref, code_ref, gate_ref, up_ref, down_ref, out_ref, rows_ref, scale_ref):
-    index = pl.program_id(0)
-    experts = pl.num_programs(0)
-    tiles, count, _, depth = rows_ref.shape
-    span = count * pitch
-    tokens = x_ref.shape[0] // tiles
-
-    def hits(tile, choice):
-        wanted = code_ref[tile, pl.ds(choice, 1), :]
+def flipped(value, mask, bits):
+    total = 0
+    for bit in range(bits):
+        digit = (value // (1 << bit)) % 2
+        total = total + (1 << bit) * (1 - digit if mask >> bit & 1 else digit)
+    return total
+
+
+def mixture_kernel(
+    pitch,
+    x_ref,
+    middle_ref,
+    code_ref,
+    gate_ref,
+    up_ref,
+    down_ref,
+    out_ref,
+    tok,
+    hot,
+    hot_turned,
+    scale,
+    picked,
+    gate_sum,
+    up_sum,
+    active,
+    gate_buf,
+    up_buf,
+    down_buf,
+    core_land,
+    diag_land,
+    side_land,
+    line_land,
+    own_sum,
+    line_sem,
+    side_sem,
+    diag_sem,
+    core_sem,
+    pass_sem,
+    core_back,
+    diag_back,
+    side_back,
+    line_back,
+    send_back,
+    weight_sem,
+    down_sem,
+):
+    groups, sets = lax.axis_size("sp"), lax.axis_size("tp")
+    lines = sets // 4
+    bits = lines.bit_length() - 1
+    chunks, pairs, _, rows, width = tok.shape
+    experts = picked.shape[0]
+    tiles, span, tokens = hot.shape
+    per_tile = tokens // (2 * rows)
+    half = lines // 2
+    sp, tp = lax.axis_index("sp"), lax.axis_index("tp")
+    core, row, line = tp % 2, (tp // 2) % 2, tp // 4
+
+    def device(side, at, up, half_chip):
+        return {"sp": side, "tp": at * 4 + up * 2 + half_chip}
+
+    def pair_of(side, at, up):
+        return side * (sets // 2) + at * 2 + up
+
+    at_line = [flipped(line, m, bits) for m in range(lines)]
+    own = [pair_of(sp, at_line[m], row) for m in range(lines)]
+    by_x = [pair_of(1 - sp, at_line[m], row) for m in range(lines)]
+    by_y = [pair_of(sp, at_line[m], 1 - row) for m in range(lines)]
+    by_xy = [pair_of(1 - sp, at_line[m], 1 - row) for m in range(lines)]
+    x_device = device(1 - sp, line, row, core)
+    y_device = device(sp, line, 1 - row, core)
+    core_device = device(sp, line, row, 1 - core)
+    line_device = [device(sp, at_line[m], row, core) for m in range(lines)]
+
+    barrier = pltpu.get_barrier_semaphore()
+    everyone = [x_device, y_device, core_device] + line_device[1:]
+    for one in everyone:
+        pl.semaphore_signal(barrier, inc=1, device_id=one, device_id_type=MESH)
+
+    def weight_copies(chunk):
+        part = pl.ds(chunk * width, width)
+        slot = chunk % 2
+        return (
+            pltpu.make_async_copy(
+                gate_ref.at[:, part, :], gate_buf.at[slot], weight_sem.at[slot, 0]
+            ),
+            pltpu.make_async_copy(up_ref.at[:, part, :], up_buf.at[slot], weight_sem.at[slot, 1]),
+        )
+
+    def down_copy(chunk):
+        part = pl.ds(chunk * width, width)
+        return pltpu.make_async_copy(
+            down_ref.at[:, :, part], down_buf.at[chunk], down_sem.at[chunk]
+        )
+
+    for chunk in range(min(2, chunks)):
+        for copy in weight_copies(chunk):
+            copy.start()
+
+    pl.semaphore_wait(barrier, len(everyone))
+
+    def push(source, target, send, receive, where):
+        pltpu.make_async_remote_copy(
+            src_ref=source,
+            dst_ref=target,
+            send_sem=send,
+            recv_sem=receive,
+            device_id=where,
+            device_id_type=MESH,
+        ).start()
+
+    def settle(view, sem):
+        pltpu.make_async_copy(view, view, sem).wait()
+
+    def spot(chunk, pair):
+        return tok.at[chunk, pair, core]
+
+    def share(chunk, pair, part):
+        push(
+            spot(chunk, pair),
+            spot(chunk, pair),
+            pass_sem.at[chunk, part],
+            core_sem.at[chunk],
+            core_device,
+        )
+
+    def send_own(chunk):
+        source = x_ref.at[:, pl.ds(chunk * width, width)]
+        target = spot(chunk, own[0])
+        early = pass_sem.at[chunk, 0]
+        for m in range(1, lines):
+            push(source, target, early, line_sem.at[chunk, m - 1], line_device[m])
+        push(source, target, early, side_sem.at[chunk, 0, 0], x_device)
+        push(source, target, early, side_sem.at[chunk, 1, 0], y_device)
+        push(source, target, early, core_sem.at[chunk], core_device)
+
+    def pass_line(chunk):
+        for m in range(1, lines):
+            settle(spot(chunk, own[m]), line_sem.at[chunk, m - 1])
+            here = spot(chunk, own[m])
+            early = pass_sem.at[chunk, 0]
+            push(here, here, early, side_sem.at[chunk, 0, m], x_device)
+            push(here, here, early, side_sem.at[chunk, 1, m], y_device)
+            share(chunk, own[m], 0)
+
+    def pass_side(chunk):
+        for m in [*range(half, lines), *range(half)]:
+            turn = ((0, by_x), (1, by_y)) if m >= half else ((1, by_y), (0, by_x))
+            for axis, column in turn:
+                here = spot(chunk, column[m])
+                settle(here, side_sem.at[chunk, axis, m])
+                late = pass_sem.at[chunk, 1]
+                if axis == 0 and m >= half:
+                    push(here, here, late, diag_sem.at[chunk, m], y_device)
+                if axis == 1 and m < half:
+                    push(here, here, late, diag_sem.at[chunk, m], x_device)
+                share(chunk, column[m], 1)
+
+    def pass_diag(chunk):
+        for m in range(lines):
+            settle(spot(chunk, by_xy[m]), diag_sem.at[chunk, m])
+            share(chunk, by_xy[m], 1)
+
+    def finish(chunk):
+        settle(tok.at[chunk, :, 0], core_sem.at[chunk])
+
+    for chunk in range(chunks):
+        send_own(chunk)
+    for chunk in range(chunks):
+        tok[chunk, own[0], core] = x_ref[:, chunk * width : (chunk + 1) * width]
+
+    for tile in range(tiles):
         slots = lax.broadcasted_iota(jnp.int32, (span, tokens), 0)
-        return slots == wanted.astype(jnp.int32)
-
-    @pl.when(index == 0)
-    def _():
+        first = slots == code_ref[tile, pl.ds(0, 1), :].astype(jnp.int32)
+        second = slots == code_ref[tile, pl.ds(1, 1), :].astype(jnp.int32)
+        chosen = jnp.where(first | second, 1.0, 0.0)
+        hot[tile] = chosen.astype(jnp.bfloat16)
+        hot_turned[tile] = chosen.T.astype(jnp.bfloat16)
+        portion = jnp.where(first, code_ref[tile, pl.ds(2, 1), :], 0.0) + jnp.where(
+            second, code_ref[tile, pl.ds(3, 1), :], 0.0
+        )
+        scale[:, tile * pitch : (tile + 1) * pitch, :] = jnp.sum(
+            portion, axis=1, keepdims=True
+        ).reshape(experts, pitch, 1)
+
+    def pick(chunk, tile):
+        block = tok[chunk, tile * per_tile : (tile + 1) * per_tile].reshape(tokens, width)
+        found = jnp.dot(hot[tile], block, preferred_element_type=jnp.float32)
+        picked[:, tile * pitch : (tile + 1) * pitch, :] = found.astype(jnp.bfloat16).reshape(
+            experts, pitch, width
+        )
+
+    def hidden(chunk, low, high):
+        slot = chunk % 2
+
+        def one(expert, carry):
+            block = picked[expert]
+            gate = jnp.dot(block, gate_buf[slot, expert], preferred_element_type=jnp.float32)
+            upward = jnp.dot(block, up_buf[slot, expert], preferred_element_type=jnp.float32)
+            if chunk > 0:
+                gate = gate + gate_sum[expert]
+                upward = upward + up_sum[expert]
+            if chunk + 1 < chunks:
+                gate_sum[expert] = gate
+                up_sum[expert] = upward
+            else:
+                active[expert] = clamped_unit(gate, upward).astype(jnp.bfloat16)
+            return carry
+
+        lax.fori_loop(low, high, one, 0, unroll=2)
+
+    pass_line(0)
+    if chunks > 1:
+        pass_line(1)
+    pass_side(0)
+    if chunks > 2:
+        pass_line(2)
+    pass_diag(0)
+    for chunk in range(chunks):
+        finish(chunk)
         for tile in range(tiles):
-            first, second = hits(tile, 0), hits(tile, 1)
-            chosen = jnp.where(first | second, 1.0, 0.0).astype(jnp.bfloat16)
-            picked = jnp.dot(
-                chosen,
-                x_ref[pl.ds(tile * tokens, tokens), :],
-                preferred_element_type=jnp.float32,
+            pick(chunk, tile)
+        if chunk + 1 < chunks:
+            pass_side(chunk + 1)
+        for copy in weight_copies(chunk):
+            copy.wait()
+        hidden(chunk, 0, experts // 2)
+        if chunk + 3 < chunks:
+            pass_line(chunk + 3)
+        if chunk + 1 < chunks:
+            pass_diag(chunk + 1)
+        hidden(chunk, experts // 2, experts)
+        if chunk + 2 < chunks:
+            for copy in weight_copies(chunk + 2):
+                copy.start()
+        if chunk == 0:
+            for later in range(chunks):
+                down_copy(later).start()
+
+    for chunk in range(chunks):
+        settle(tok.at[chunk, : pairs - 1, 0], pass_sem.at[chunk, 0])
+        settle(tok.at[chunk, :, 0], pass_sem.at[chunk, 1])
+
+    def lower(chunk):
+        down_copy(chunk).wait()
+
+        def one(expert, carry):
+            result = jnp.dot(
+                active[expert], down_buf[chunk, expert], preferred_element_type=jnp.float32
+            )
+            picked[expert] = (result * scale[expert]).astype(jnp.bfloat16)
+            return carry
+
+        lax.fori_loop(0, experts, one, 0, unroll=2)
+        for tile in range(tiles):
+            block = picked[:, tile * pitch : (tile + 1) * pitch, :].reshape(span, width)
+            total = jnp.dot(hot_turned[tile], block, preferred_element_type=jnp.float32)
+            tok[chunk, tile * per_tile : (tile + 1) * per_tile] = total.astype(
+                jnp.bfloat16
+            ).reshape(per_tile, 2, rows, width)
+
+    def meet_core(chunk):
+        push(
+            tok.at[chunk, :, 1 - core],
+            core_land.at[chunk],
+            send_back.at[chunk, 0],
+            core_back.at[chunk],
+            core_device,
+        )
+
+    def add_core(chunk, pair):
+        tok[chunk, pair, core] = (
+            tok[chunk, pair, core].astype(jnp.float32) + core_land[chunk, pair].astype(jnp.float32)
+        ).astype(jnp.bfloat16)
+
+    def back_diag(chunk):
+        settle(core_land.at[chunk], core_back.at[chunk])
+        send = send_back.at[chunk, 1]
+        for m in range(lines):
+            add_core(chunk, by_xy[m])
+            push(
+                spot(chunk, by_xy[m]),
+                diag_land.at[chunk, m],
+                send,
+                diag_back.at[chunk, m],
+                y_device if m >= half else x_device,
+            )
+        for m in range(lines):
+            axis, column, where = (1, by_y, y_device) if m >= half else (0, by_x, x_device)
+            add_core(chunk, column[m])
+            push(
+                spot(chunk, column[m]),
+                side_land.at[chunk, axis, m],
+                send,
+                side_back.at[chunk, axis, m],
+                where,
+            )
+        for m in range(lines):
+            add_core(chunk, (by_x if m >= half else by_y)[m])
+            add_core(chunk, own[m])
+
+    def back_side(chunk):
+        for m in range(lines):
+            axis, column, where = (0, by_x, x_device) if m >= half else (1, by_y, y_device)
+            settle(diag_land.at[chunk, m], diag_back.at[chunk, m])
+            tok[chunk, column[m], core] = (
+                tok[chunk, column[m], core].astype(jnp.float32)
+                + diag_land[chunk, m].astype(jnp.float32)
             ).astype(jnp.bfloat16)
-            rows_ref[tile] = picked.reshape(count, pitch, depth)
-            share = jnp.where(first, code_ref[tile, pl.ds(2, 1), :], 0.0) + jnp.where(
-                second, code_ref[tile, pl.ds(3, 1), :], 0.0
+            push(
+                spot(chunk, column[m]),
+                side_land.at[chunk, axis, m],
+                send_back.at[chunk, 2],
+                side_back.at[chunk, axis, m],
+                where,
             )
-            scale_ref[tile] = jnp.sum(share, axis=1, keepdims=True).reshape(count, pitch, 1)
-
-    rows = rows_ref[:, index].reshape(tiles * pitch, depth)
-    gate = jnp.dot(rows, gate_ref[0], preferred_element_type=jnp.float32)
-    upward = jnp.dot(rows, up_ref[0], preferred_element_type=jnp.float32)
-    activated = clamped_unit(gate, upward).astype(jnp.bfloat16)
-    result = jnp.dot(activated, down_ref[0], preferred_element_type=jnp.float32)
-    scaled = result * scale_ref[:, index].reshape(tiles * pitch, 1)
-    rows_ref[:, index] = scaled.astype(jnp.bfloat16).reshape(tiles, pitch, depth)
-
-    @pl.when(index == experts - 1)
-    def _():
-        for tile in range(tiles):
-            chosen = jnp.where(hits(tile, 0) | hits(tile, 1), 1.0, 0.0).astype(jnp.bfloat16)
-            out_ref[pl.ds(tile * tokens, tokens), :] = lax.dot_general(
-                chosen,
-                rows_ref[tile].reshape(span, depth),
-                (((0,), (0,)), ((), ())),
-                preferred_element_type=jnp.float32,
-            ).astype(jnp.bfloat16)
-
-
-def run_experts(tokens, codes, gate_weight, up_weight, down_weight, pitch):
+
+    def back_line(chunk):
+        for m in [*range(1, lines), 0]:
+            total = tok[chunk, own[m], core].astype(jnp.float32)
+            for axis in range(2):
+                settle(side_land.at[chunk, axis, m], side_back.at[chunk, axis, m])
+                total = total + side_land[chunk, axis, m].astype(jnp.float32)
+            if m == 0:
+                own_sum[chunk] = total
+                continue
+            tok[chunk, own[m], core] = total.astype(jnp.bfloat16)
+            push(
+                spot(chunk, own[m]),
+                line_land.at[chunk, m - 1],
+                send_back.at[chunk, 3],
+                line_back.at[chunk, m - 1],
+                line_device[m],
+            )
+
+    def close(chunk):
+        total = own_sum[chunk]
+        for m in range(1, lines):
+            settle(line_land.at[chunk, m - 1], line_back.at[chunk, m - 1])
+            total = total + line_land[chunk, m - 1].astype(jnp.float32)
+        part = slice(chunk * width, (chunk + 1) * width)
+        out_ref[:, part] = (middle_ref[:, part].astype(jnp.float32) + total).astype(jnp.bfloat16)
+
+    stages = (back_diag, back_side, back_line, close)
+    for step in range(chunks + len(stages)):
+        if step < chunks:
+            lower(step)
+            meet_core(step)
+        for number, stage in enumerate(stages):
+            chunk = step - 1 - number
+            if 0 <= chunk < chunks:
+                stage(chunk)
+    for chunk in range(chunks):
+        settle(core_land.at[chunk], send_back.at[chunk, 0])
+        settle(tok.at[chunk, : 2 * lines, 0], send_back.at[chunk, 1])
+        settle(tok.at[chunk, :lines, 0], send_back.at[chunk, 2])
+        settle(tok.at[chunk, : lines - 1, 0], send_back.at[chunk, 3])
+
+
+def run_mixture(
+    tokens, middle, codes, gate_weight, up_weight, down_weight, pitch, chunks, collective_id
+):
     experts, depth, units = gate_weight.shape
-    tiles = codes.shape[0]
+    tiles, _, tile_tokens = codes.shape
+    rows = tokens.shape[0]
+    groups, sets = lax.axis_size("sp"), lax.axis_size("tp")
+    pairs, lines = groups * sets // 2, sets // 4
+    width = depth // chunks
+    span = experts * pitch
+    narrow, wide = jnp.bfloat16, jnp.float32
+    anywhere = pl.BlockSpec(memory_space=pl.ANY)
+    dma = pltpu.SemaphoreType.DMA
     return pl.pallas_call(
-        functools.partial(expert_kernel, pitch),
-        grid=(experts,),
+        functools.partial(mixture_kernel, pitch),
         out_shape=jax.ShapeDtypeStruct(tokens.shape, jnp.bfloat16),
-        in_specs=[
-            pl.BlockSpec(tokens.shape, lambda i: (0, 0)),
-            pl.BlockSpec(codes.shape, lambda i: (0, 0, 0)),
-            pl.BlockSpec((1, depth, units), lambda i: (i, 0, 0)),
-            pl.BlockSpec((1, depth, units), lambda i: (i, 0, 0)),
-            pl.BlockSpec((1, units, depth), lambda i: (i, 0, 0)),
-        ],
-        out_specs=pl.BlockSpec(tokens.shape, lambda i: (0, 0)),
+        in_specs=[VMEM, VMEM, VMEM, anywhere, anywhere, anywhere],
+        out_specs=VMEM,
         scratch_shapes=[
-            pltpu.VMEM((tiles, experts, pitch, depth), jnp.bfloat16),
-            pltpu.VMEM((tiles, experts, pitch, 1), jnp.float32),
+            pltpu.VMEM((chunks, pairs, 2, rows, width), narrow),
+            pltpu.VMEM((tiles, span, tile_tokens), narrow),
+            pltpu.VMEM((tiles, tile_tokens, span), narrow),
+            pltpu.VMEM((experts, tiles * pitch, 1), wide),
+            pltpu.VMEM((experts, tiles * pitch, width), narrow),
+            pltpu.VMEM((experts, tiles * pitch, units), wide),
+            pltpu.VMEM((experts, tiles * pitch, units), wide),
+            pltpu.VMEM((experts, tiles * pitch, units), narrow),
+            pltpu.VMEM((2, experts, width, units), narrow),
+            pltpu.VMEM((2, experts, width, units), narrow),
+            pltpu.VMEM((chunks, experts, units, width), narrow),
+            pltpu.VMEM((chunks, pairs, rows, width), narrow),
+            pltpu.VMEM((chunks, lines, rows, width), narrow),
+            pltpu.VMEM((chunks, 2, lines, rows, width), narrow),
+            pltpu.VMEM((chunks, lines - 1, rows, width), narrow),
+            pltpu.VMEM((chunks, rows, width), wide),
+            dma((chunks, lines - 1)),
+            dma((chunks, 2, lines)),
+            dma((chunks, lines)),
+            dma((chunks,)),
+            dma((chunks, 2)),
+            dma((chunks,)),
+            dma((chunks, lines)),
+            dma((chunks, 2, lines)),
+            dma((chunks, lines - 1)),
+            dma((chunks, 4)),
+            dma((2, 2)),
+            dma((chunks,)),
         ],
         compiler_params=pltpu.CompilerParams(
-            dimension_semantics=("arbitrary",), vmem_limit_bytes=36 << 20
+            collective_id=collective_id, has_side_effects=True, vmem_limit_bytes=63 << 20
         ),
-        name="run_experts",
-    )(tokens, codes, gate_weight, up_weight, down_weight)
+        name="run_mixture",
+    )(tokens, middle, codes, gate_weight, up_weight, down_weight)
 
 
 def attended_heads(queries, nope, keys, turned, values, allowed, scale):
@@ -683,20 +954,14 @@
     own_residual = lax.dynamic_slice_in_dim(residual, own_start, own_rows, 0)
     middle = (own_residual.astype(jnp.float32) + projected).astype(jnp.bfloat16)
     normed = rms_scaled(middle, expert_gain).astype(jnp.bfloat16)
-    ladder = rest[::-1]
-    one = tuple(ladder + across + first + core)
-    two = tuple(ladder + first + across + core)
-    tokens = gather_blocks(normed, (one, two, one, two), sets, groups * sets, 2)
-
     tiles = total // TILE_TOKENS
     codes = jnp.swapaxes(routes, 0, 1).reshape(8, total)
     shift = jnp.array([1.0, 1.0, 0.0, 0.0, 1.0, 1.0, 0.0, 0.0], jnp.float32)
     codes = codes - (shift * (me * local_experts * pitch).astype(jnp.float32))[:, None]
     codes = jnp.swapaxes(codes.reshape(8, tiles, TILE_TOKENS), 0, 1)
-    mixed = run_experts(tokens, codes, gate_weight, up_weight, down_weight, pitch)
-    one, two = one[::-1], two[::-1]
-    mixture = scatter_blocks(mixed, (one, two, one, two), sets, groups * sets, 3)
-    return (middle.astype(jnp.float32) + mixture).astype(jnp.bfloat16)
+    return run_mixture(
+        normed, middle, codes, gate_weight, up_weight, down_weight, pitch, CHUNKS, 2
+    )
 
 
 def solution(mesh):
@@ -722,7 +987,7 @@
     )
     out_specs = P(("sp", "tp"), None)
     groups, sets = mesh.shape["sp"], mesh.shape["tp"]
-    small = groups == 2 and sets & (sets - 1) == 0 and sets > 2
+    small = groups == 2 and sets & (sets - 1) == 0 and sets > 4
 
     def body(*arguments):
         fits = small and arguments[2].shape[0] * groups <= 1024

time: 166 us -> 139 us (0.84)
  Pallas kernels: 137 us -> 108 us
    pallas_call x2 -> x1, Pallas kernels: 61.2 us -> 25.1 us  [scatter_blocks(): pl.pallas_call(functools.partial(scatter_kernel, orders, width, rows), ou...]
    pallas_call x2 -> x1, Pallas kernels: 60.9 us -> 68.1 us  [run_mixture(): pl.pallas_call(functools.partial(mixture_kernel, pitch), out_shape=jax.Sh...]
    unnamed x32 -> x35, local copies, waits for them, and re-layouts: 5.86 us -> 7.43 us
where the time goes in v1:
time: 139 us; the launch traced here: 138 us
  Pallas kernels  108 us (78%)
  other arithmetic  10.7 us (8%)
  local copies, waits for them, and re-layouts  10.6 us (8%)
  matrix products  8.71 us (6%)
    pallas_call x1, Pallas kernels, run_mixture(): pl.pallas_call(functools.partial(mixture_kernel, pitch), out_shape=jax.Sh...  68.1 us
    pallas_call x1, Pallas kernels, scatter_blocks(): pl.pallas_call(functools.partial(scatter_kernel, orders, width, rows), ou...  25.1 us
    pallas_call x1, Pallas kernels, exchange(): pl.pallas_call(exchange_kernel, out_shape=tuple((jax.ShapeDtypeStruct((2,...  14.8 us
    unnamed x35, local copies, waits for them, and re-layouts  7.43 us
    dot_general x2, matrix products, attended_heads(): jnp.einsum('hqk,khd->hqd', weights.astype(jnp.bfloat16), value_rows, pref...  5.09 us

profile of v1, /device:TPU:0, one launch (start us, length us, event | category | flops | bytes accessed | tf_op | source)
XLA Modules:
  0.0 138.2 jit_solution(11517763123611988779)
XLA Ops:
  0.0 0.7 broadcast_multiply_fusion
  0.7 0.7 reduce_max.27
  1.5 0.7 fusion.60
  2.4 0.9 slice.44
  3.3 0.9 slice.51
  4.2 0.9 copy.26
  5.1 0.7 pad.4.turn_ref
  5.8 0.8 slice_convert_fusion
  6.8 0.8 copy.27
  9.2 14.8 %exchange.1 = (bf16[2,512,512]{2,1,0:T(8,128)(2,1)}, bf16[2,512,128]{2,1,0:T(8,128)(2,1)}, f32[2,8,512]{2,1,0:T(8,128)}) custom-call(bf16[512,512]{1,0:T(8,128)(2,1)} %latent_ref.1, bf16[512,128]{1,0:T(8,128)(2,1)} %pad.4.turn_ref, f32[8,512]{1,0:T(8,128)} %pad_maximum_fusion.route_ref), custom_call_target="tpu_custom_call" | custom-call | tf_op jit(solution)/shard_map/exchange/pallas_call | solution.py:433
  24.0 1.1 copy.30
  25.1 1.4 %subtract_bitcast_fusion.code_ref = f32[4,8,256]{2,1,0:T(8,128)} fusion(f32[8,4,256]{2,0,1:T(8,128)} %bitcast.66, f32[8]{0:T(128)S(1)} %broadcast_multiply_fusion), kind=kLoop, calls=%fused_computation.85 | loop fusion | flops 8192 | bytes 65568 | tf_op jit(solution)/shard_map/transpose | solution.py:961
  26.6 1.5 %multiply_reduce_fusion = f32[2,512]{1,0:T(2,128)S(1)} fusion(bf16[2,512,512]{2,1,0:T(8,128)(2,1)} %get-tuple-element.8), kind=kLoop, calls=%fused_computation.8 | loop fusion | flops 1571840 | bytes 1052672 | tf_op jit(solution)/shard_map/reduce_sum | solution.py:38
  30.4 1.3 copy-done.4
  32.3 2.7 %fusion.9 = bf16[512,128]{1,0:T(8,128)(2,1)S(1)} fusion(bf16[1024,512]{1,0:T(8,128)(2,1)S(1)} %fusion.1, bf16[512,128]{1,0:T(8,128)(2,1)S(1)} %copy-done.14, f32[512,1024]{1,0:T(8,128)} %copy-done.4, f32[512]{0:T(512)S(1)} %get-tuple-element.21, f32[512]{0:T(512)S(1)} %fusion.4), kind=kOutput, calls=%fused_computation.19 | convolution fusion | flops 269746176 | bytes 3411968 | tf_op jit(solution)/shard_map/hqk,khd->hqd/dot_general | solution.py:874
  35.7 1.4 copy-done.2
  37.5 2.4 %fusion.11 = bf16[512,64]{0,1:T(8,128)(2,1)S(1)} fusion(bf16[1024,512]{1,0:T(8,128)(2,1)S(1)} %fusion.1, bf16[512,64]{0,1:T(8,128)(2,1)S(1)} %copy-done.9, f32[512,1024]{1,0:T(8,128)} %copy-done.2, f32[512]{0:T(512)S(1)} %get-tuple-element.23, f32[512]{0:T(512)S(1)} %fusion.2), kind=kOutput, calls=%fused_computation.24 | convolution fusion | flops 135397376 | bytes 3280896 | tf_op jit(solution)/shard_map/hqk,khd->hqd/dot_general | solution.py:874
  39.9 0.7 fusion.68
  40.8 0.7 add_convert_fusion.x_ref
  41.6 25.1 %scatter_blocks.1 = f32[32,2048]{1,0:T(8,128)S(1)} custom-call(bf16[512,2048]{1,0:T(8,128)(2,1)S(1)} %add_convert_fusion.x_ref), custom_call_target="tpu_custom_call" | custom-call | tf_op jit(solution)/shard_map/scatter_blocks/pallas_call | solution.py:353
  66.7 1.1 fusion.20
  67.8 0.8 fusion.22.x_ref
  68.6 68.1 %run_mixture.1 = bf16[32,2048]{1,0:T(8,128)(2,1)} custom-call(bf16[32,2048]{1,0:T(8,128)(2,1)} %fusion.22.x_ref, bf16[32,2048]{1,0:T(8,128)(2,1)} %copy-done.5, f32[4,8,256]{2,1,0:T(8,128)} %subtract_bitcast_fusion.code_ref, bf16[16,2048,256]{2,1,0:T(8,128)(2,1)} %gate_ref.1, bf16[16,2048,256]{2,1,0:T(8,128)(2,1)} %up_ref.1, bf16[16,256,2048]{2,1,0:T(8,128)(2,1)} %down_ref.1), custom_call_target="tpu_custom_call" | custom-call | tf_op jit(solution)/shard_map/run_mixture/pallas_call | solution.py:821
  136.7 1.6 %copy.33 = bf16[32,2048]{1,0:T(8,128)(2,1)} copy(bf16[32,2048]{1,0:T(8,128)(2,1)} %run_mixture.1) | data formatting | bytes 262144
  (55 shorter events, 6.2 us)
Async XLA Ops:
  0.0 39.9 %copy-start = (bf16[128,2048]{1,0:T(8,128)(2,1)S(1)}, bf16[128,2048]{1,0:T(8,128)(2,1)}, u32[]{:S(2)}) copy-start(bf16[128,2048]{1,0:T(8,128)(2,1)} %param.29) | copy-start | bytes 1572868
  0.0 8.5 %copy-start.10 = (f32[512,2]{0,1:T(2,128)S(1)}, f32[512,2]{0,1:T(2,128)}, u32[]{:S(2)}) copy-start(f32[512,2]{0,1:T(2,128)} %param.33) | copy-start | bytes 12292
  0.0 8.5 %copy-start.11 = (s32[512,2]{0,1:T(2,128)S(1)}, s32[512,2]{0,1:T(2,128)}, u32[]{:S(2)}) copy-start(s32[512,2]{0,1:T(2,128)} %param.32) | copy-start | bytes 12292
  4.2 23.9 %copy-start.13 = (f32[512]{0:T(512)S(1)}, f32[512]{0:T(512)}, u32[]{:S(2)}) copy-start(f32[512]{0:T(512)} %param.23) | copy-start | bytes 6148
  24.0 4.2 %copy-start.3 = (bf16[2,512,512]{2,1,0:T(8,128)(2,1)S(1)}, bf16[2,512,512]{2,1,0:T(8,128)(2,1)}, u32[]{:S(2)}) copy-start(bf16[2,512,512]{2,1,0:T(8,128)(2,1)} %get-tuple-element.8) | copy-start | bytes 3145732
  24.0 4.8 %copy-start.8 = (bf16[512,64]{0,1:T(8,128)(2,1)S(1)}, bf16[512,64]{0,1:T(8,128)(2,1)}, u32[]{:S(2)}) copy-start(bf16[512,64]{0,1:T(8,128)(2,1)} %param.24) | copy-start | bytes 196612
  28.1 1.2 copy-start.7
  30.4 1.4 copy-start.4
  30.4 1.9 %copy-start.14 = (bf16[512,128]{1,0:T(8,128)(2,1)S(1)}, bf16[512,128]{1,0:T(8,128)(2,1)}, u32[]{:S(2)}) copy-start(bf16[512,128]{1,0:T(8,128)(2,1)} %param.27) | copy-start | bytes 393220
  35.0 2.5 %copy-start.9 = (bf16[512,64]{0,1:T(8,128)(2,1)S(1)}, bf16[512,64]{0,1:T(8,128)(2,1)}, u32[]{:S(2)}) copy-start(bf16[512,64]{0,1:T(8,128)(2,1)} %param.25) | copy-start | bytes 196612
  35.6 1.4 copy-start.2
  39.9 1.0 copy-start.6
  41.6 26.2 %copy-start.12 = (f32[2048]{0:T(1024)S(1)}, f32[2048]{0:T(1024)}, u32[]{:S(2)}) copy-start(f32[2048]{0:T(1024)} %param.31) | copy-start | bytes 24580
  67.8 0.8 copy-start.5
  68.6 69.7 %copy-start.1 = (bf16[128,2048]{1,0:T(8,128)(2,1)S(1)}, bf16[128,2048]{1,0:T(8,128)(2,1)}, u32[]{:S(2)}) copy-start(bf16[128,2048]{1,0:T(8,128)(2,1)} %param.29) | copy-start | bytes 1572868

commit v2 on v1

--- a/solution.py
+++ b/solution.py
@@ -2,6 +2,7 @@
 
 import jax
 import jax.numpy as jnp
+import numpy as np
 from jax import lax
 from jax.experimental import pallas as pl
 from jax.experimental.pallas import tpu as pltpu
@@ -226,233 +227,372 @@
 CHUNKS = 4
 
 
-def places_of(axes):
-    return {axis: lax.axis_index(axis) for axis in axes}
-
-
-def bit_of(place, step):
-    axis, mask = step
-    return (place[axis] // mask) % 2
-
-
-def partner_of(place, step):
-    axis, mask = step
-    return {axis: place[axis] + mask * (1 - 2 * bit_of(place, step))}
-
-
-def greet(place, steps):
-    barrier = pltpu.get_barrier_semaphore()
-    for step in steps:
-        pl.semaphore_signal(
-            barrier, inc=1, device_id=partner_of(place, step), device_id_type=MESH
-        )
-    pl.semaphore_wait(barrier, len(steps))
-
-
-def cube_steps(sp, tp):
-    core = [("tp", 1)] if tp > 1 else []
-    first = [("tp", 2)] if tp > 2 else []
-    rest = [("tp", 1 << i) for i in range(2, tp.bit_length() - 1)]
-    across = [("sp", 1 << i) for i in range(sp.bit_length() - 1)]
-    return core, first, rest, across
-
-
-def weight_of(step, widths):
-    axis, mask = step
-    return mask * (widths if axis == "sp" else 1)
-
-
-def base_of(place, fixed, width):
-    total = jnp.int32(0)
-    for step in fixed:
-        total = total + bit_of(place, step) * weight_of(step, width)
-    return total
-
-
-def offsets_of(free, width):
-    found = [0]
-    for step in free:
-        found = found + [one + weight_of(step, width) for one in found]
-    return found
-
-
-def block_rows_of(index, rows):
-    return pl.ds(pl.multiple_of(index * rows, rows), rows)
-
-
-def scatter_kernel(
-    orders, width, rows, x_ref, out_ref, total_ref, landing_ref, send_sem, recv_sem
-):
-    place = places_of(("sp", "tp"))
-    stages = len(orders[0])
-    cols = x_ref.shape[1] // len(orders)
-    greet(place, orders[0])
-    spots = [0]
-    for number in range(stages):
-        spots.append(spots[-1] + (1 << (stages - 1 - number)))
-
-    def columns(part):
-        return pl.ds(part * cols, cols)
-
-    def start(part, number):
-        order = orders[part]
-        step = order[number]
-        source = x_ref if number == 0 else total_ref
-        base = base_of(place, order[:number], width)
-        base = base + (1 - bit_of(place, step)) * weight_of(step, width)
-        for slot, offset in enumerate(offsets_of(order[number + 1 :], width)):
-            pltpu.make_async_remote_copy(
-                src_ref=source.at[block_rows_of(base + offset, rows), columns(part)],
-                dst_ref=landing_ref.at[pl.ds((spots[number] + slot) * rows, rows), columns(part)],
-                send_sem=send_sem.at[part, number],
-                recv_sem=recv_sem.at[part, number],
-                device_id=partner_of(place, step),
-                device_id_type=MESH,
-            ).start()
-
-    def drain(part, number, sem):
-        count = 1 << (stages - 1 - number)
-        whole = landing_ref.at[pl.ds(spots[number] * rows, count * rows), columns(part)]
-        pltpu.make_async_copy(whole, whole, sem.at[part, number]).wait()
-
-    def add(part, number):
-        order = orders[part]
-        source = x_ref if number == 0 else total_ref
-        base = base_of(place, order[: number + 1], width)
-        for slot, offset in enumerate(offsets_of(order[number + 1 :], width)):
-            here = block_rows_of(base + offset, rows)
-            there = pl.ds((spots[number] + slot) * rows, rows)
-            value = source[here, columns(part)].astype(jnp.float32) + landing_ref[
-                there, columns(part)
-            ].astype(jnp.float32)
-            if number + 1 < stages:
-                total_ref[here, columns(part)] = value.astype(total_ref.dtype)
-            else:
-                out_ref[:, columns(part)] = value
-
-    for part in range(len(orders)):
-        start(part, 0)
-    for wave in range(stages + 1):
-        for part in range(len(orders)):
-            number = wave - part // 2 % 2
-            if number < 0 or number >= stages:
-                continue
-            drain(part, number, recv_sem)
-            add(part, number)
-            if number + 1 < stages:
-                start(part, number + 1)
-    for part in range(len(orders)):
-        for number in range(stages):
-            drain(part, number, send_sem)
-
-
-def scatter_blocks(x, orders, width, count, collective_id):
-    rows = x.shape[0] // count
-    depth = x.shape[1]
-    parts, stages = len(orders), len(orders[0])
-    return pl.pallas_call(
-        functools.partial(scatter_kernel, orders, width, rows),
-        out_shape=jax.ShapeDtypeStruct((rows, depth), jnp.float32),
-        in_specs=[VMEM],
-        out_specs=VMEM,
-        scratch_shapes=[
-            pltpu.VMEM(x.shape, x.dtype),
-            pltpu.VMEM(((count - 1) * rows, depth), x.dtype),
-            pltpu.SemaphoreType.DMA((parts, stages)),
-            pltpu.SemaphoreType.DMA((parts, stages)),
-        ],
-        compiler_params=pltpu.CompilerParams(
-            collective_id=collective_id, has_side_effects=True, vmem_limit_bytes=16 << 20
-        ),
-        name="scatter_blocks",
-    )(x)
-
-
-def exchange_kernel(latent_ref, turn_ref, route_ref, l_out, t_out, r_out, send_sem, recv_sem, own_sem):
-    place = places_of(("sp", "tp"))
-    across, core = ("sp", 1), ("tp", 1)
-    greet(place, (across, core))
-    half = latent_ref.shape[0] // 2
-    side = bit_of(place, core)
-    me = place["sp"]
-    other = 1 - me
-    pairs = ((latent_ref, l_out), (turn_ref, t_out))
-    mine = pl.ds(pl.multiple_of(side * half, half), half)
-    crossing = []
-    for number, (source, target) in enumerate(pairs):
-        crossing.append(
-            pltpu.make_async_remote_copy(
-                src_ref=source.at[mine, :],
-                dst_ref=target.at[me, mine, :],
-                send_sem=send_sem.at[number],
-                recv_sem=recv_sem.at[number],
-                device_id=partner_of(place, across),
-                device_id_type=MESH,
-            )
-        )
-    crossing.append(
-        pltpu.make_async_remote_copy(
-            src_ref=route_ref,
-            dst_ref=r_out.at[me],
-            send_sem=send_sem.at[2],
-            recv_sem=recv_sem.at[2],
-            device_id=partner_of(place, across),
-            device_id_type=MESH,
-        )
-    )
-    for copy in crossing:
-        copy.start()
-    kept = [
-        pltpu.make_async_copy(source, target.at[me], own_sem.at[number])
-        for number, (source, target) in enumerate(pairs + ((route_ref, r_out),))
-    ]
-    for copy in kept:
-        copy.start()
-    passing = []
-    for number, (source, target) in enumerate(pairs):
-        crossing[number].wait_recv()
-        spot = target.at[other, mine, :]
-        copy = pltpu.make_async_remote_copy(
-            src_ref=spot,
-            dst_ref=spot,
-            send_sem=send_sem.at[3 + number],
-            recv_sem=recv_sem.at[3 + number],
-            device_id=partner_of(place, core),
-            device_id_type=MESH,
-        )
-        copy.start()
-        passing.append(copy)
-    crossing[2].wait_recv()
-    for copy in crossing:
-        copy.wait_send()
-    for copy in kept + passing:
-        copy.wait()
-
-
-def exchange(latent, turn, route, collective_id):
-    return pl.pallas_call(
-        exchange_kernel,
-        out_shape=tuple(
-            jax.ShapeDtypeStruct((2,) + one.shape, one.dtype) for one in (latent, turn, route)
-        ),
-        in_specs=[VMEM] * 3,
-        out_specs=(VMEM,) * 3,
-        scratch_shapes=[
-            pltpu.SemaphoreType.DMA((5,)),
-            pltpu.SemaphoreType.DMA((5,)),
-            pltpu.SemaphoreType.DMA((3,)),
-        ],
-        compiler_params=pltpu.CompilerParams(collective_id=collective_id, has_side_effects=True),
-        name="exchange",
-    )(latent, turn, route)
-
-
 def flipped(value, mask, bits):
     total = 0
     for bit in range(bits):
         digit = (value // (1 << bit)) % 2
         total = total + (1 << bit) * (1 - digit if mask >> bit & 1 else digit)
     return total
+
+
+def attention_kernel(
+    pitch,
+    table_ref,
+    first_ref,
+    second_ref,
+    latent_ref,
+    rotary_ref,
+    latent_gain_ref,
+    key_first_ref,
+    value_first_ref,
+    key_second_ref,
+    value_second_ref,
+    out_first_ref,
+    out_second_ref,
+    residual_ref,
+    expert_gain_ref,
+    route_ref,
+    score_ref,
+    middle_ref,
+    normed_ref,
+    codes_ref,
+    latents,
+    rotaries,
+    queries,
+    weights,
+    residual,
+    state,
+    numerator,
+    part,
+    core_land,
+    side_land,
+    line_land,
+    total,
+    load_sem,
+    cross_sem,
+    cross_back,
+    core_sem,
+    side_sem,
+    line_sem,
+    send_sem,
+):
+    sets = lax.axis_size("tp")
+    lines = sets // 4
+    bits = lines.bit_length() - 1
+    chunks, _, _, rows, width = part.shape
+    _, seq_rows, rank = latents.shape
+    first_nope, second_nope = key_first_ref.shape[0], key_second_ref.shape[1]
+    first_width, second_width = value_first_ref.shape[0], value_second_ref.shape[1]
+    half_turn = table_ref.shape[0] // 2
+    rotary = 2 * half_turn
+    sp, tp = lax.axis_index("sp"), lax.axis_index("tp")
+    core, row, line = tp % 2, (tp // 2) % 2, tp // 4
+    wide, narrow = jnp.float32, jnp.bfloat16
+
+    at_line = [flipped(line, m, bits) for m in range(lines)]
+    x_device = {"sp": 1 - sp, "tp": tp}
+    y_device = {"sp": sp, "tp": line * 4 + (1 - row) * 2 + core}
+    core_device = {"sp": sp, "tp": line * 4 + row * 2 + 1 - core}
+    line_device = [{"sp": sp, "tp": at_line[m] * 4 + row * 2 + core} for m in range(lines)]
+
+    barrier = pltpu.get_barrier_semaphore()
+    everyone = [x_device, y_device, core_device] + line_device[1:]
+    for one in everyone:
+        pl.semaphore_signal(barrier, inc=1, device_id=one, device_id_type=MESH)
+
+    own_rows = pl.ds(pl.multiple_of(tp * rows, rows), rows)
+    loads = [
+        pltpu.make_async_copy(source, target, load_sem.at[number])
+        for number, (source, target) in enumerate(
+            (
+                (latent_ref, latents.at[0]),
+                (out_first_ref, weights.at[:first_width, :]),
+                (out_second_ref, weights.at[first_width:, :]),
+                (residual_ref.at[own_rows, :], residual),
+            )
+        )
+    ]
+    for copy in loads:
+        copy.start()
+
+    def push(source, target, send, receive, where):
+        copy = pltpu.make_async_remote_copy(
+            src_ref=source,
+            dst_ref=target,
+            send_sem=send,
+            recv_sem=receive,
+            device_id=where,
+            device_id_type=MESH,
+        )
+        copy.start()
+        return copy
+
+    def settle(view, sem):
+        pltpu.make_async_copy(view, view, sem).wait()
+
+    mine = pl.ds(pl.multiple_of(core * (seq_rows // 2), seq_rows // 2), seq_rows // 2)
+    loads[0].wait()
+    pl.semaphore_wait(barrier, len(everyone))
+
+    @pl.when(sp == 0)
+    def _():
+        push(
+            latents.at[0, mine, :],
+            latents.at[1, mine, :],
+            cross_back.at[0],
+            cross_sem.at[0],
+            x_device,
+        )
+        push(rotary_ref, rotaries, cross_back.at[1], cross_sem.at[1], x_device)
+
+    tile = 4 * rows
+    own_codes = codes_ref.at[sp]
+    scores = score_ref[...]
+    raised = jnp.exp(scores - jnp.max(scores, axis=0, keepdims=True))
+    shares = raised / jnp.sum(raised, axis=0, keepdims=True)
+    chosen = route_ref[...].astype(wide)
+    upright = jnp.concatenate([chosen] * 4, axis=0).T
+    earlier = lax.broadcasted_iota(jnp.int32, (tile, tile), 0)
+    later = lax.broadcasted_iota(jnp.int32, (tile, tile), 1)
+    counted = (earlier < later) & (earlier // rows == later // rows)
+    places = lax.broadcasted_iota(jnp.int32, (1, seq_rows), 1)
+    span_blocks = TILE_TOKENS // rows
+    spots = (places // rows % span_blocks * CAP).astype(wide)
+    lists = []
+    for choice in range(2):
+        ranks = []
+        for start in range(0, seq_rows, tile):
+            wanted = chosen[choice : choice + 1, start : start + tile]
+            same = (upright[start : start + tile, 0:1] == wanted) | (
+                upright[start : start + tile, 1:2] == wanted
+            )
+            ranks.append(jnp.sum(jnp.where(same & counted, 1.0, 0.0), axis=0, keepdims=True))
+        lists.append(
+            chosen[choice : choice + 1] * pitch + spots + jnp.concatenate(ranks, axis=1)
+        )
+    lists = jnp.concatenate(lists + [shares], axis=0)
+    own_codes[...] = jnp.concatenate([lists, lists], axis=0)
+    route_copy = push(own_codes, own_codes, cross_back.at[2], cross_sem.at[2], x_device)
+
+    own_places = pl.ds(pl.multiple_of(sp * seq_rows, seq_rows), seq_rows)
+
+    def turned(values, where):
+        cosine, sine = table_ref[:half_turn, where], table_ref[half_turn:, where]
+        upper, lower = values[:half_turn].astype(wide), values[half_turn:].astype(wide)
+        return jnp.concatenate(
+            [upper * cosine - lower * sine, lower * cosine + upper * sine], axis=0
+        )
+
+    first_end = first_nope + rotary
+    queries[:first_nope] = first_ref[:first_nope]
+    queries[first_nope:first_end] = turned(first_ref[first_nope:], own_places).astype(narrow)
+    queries[first_end : first_end + second_nope] = second_ref[:second_nope]
+    queries[first_end + second_nope :] = turned(second_ref[second_nope:], own_places).astype(narrow)
+    value_second = value_second_ref[...].astype(wide).T.astype(narrow)
+    across = (((1,), (1,)), ((), ()))
+
+    def fold(slot, rotary_values, where, causal, fresh):
+        raw = latents[slot].astype(wide)
+        root = lax.rsqrt(jnp.mean(raw * raw, axis=-1, keepdims=True) + norm_epsilon)
+        base = (raw * root * latent_gain_ref[...]).astype(narrow)
+        turned_keys = turned(rotary_values, where).T.astype(narrow)
+        if causal:
+            key_places = lax.broadcasted_iota(jnp.int32, (seq_rows, seq_rows), 0)
+            query_places = lax.broadcasted_iota(jnp.int32, (seq_rows, seq_rows), 1)
+            allowed = key_places <= query_places
+        for group in range(2):
+            if group == 0:
+                keys = lax.dot_general(base, key_first_ref[...], across, preferred_element_type=wide)
+                values = lax.dot_general(
+                    value_first_ref[...], base, across, preferred_element_type=wide
+                )
+                found = queries[:first_end]
+                spots = pl.ds(0, first_width)
+            else:
+                keys = jnp.dot(base, key_second_ref[...], preferred_element_type=wide)
+                values = lax.dot_general(value_second, base, across, preferred_element_type=wide)
+                found = queries[first_end:]
+                spots = pl.ds(first_width, second_width)
+            keys = jnp.concatenate([keys.astype(narrow), turned_keys], axis=1)
+            score = jnp.dot(keys, found, preferred_element_type=wide) * (
+                keys.shape[1] ** (-0.5)
+            )
+            if causal:
+                score = jnp.where(allowed, score, masked_score)
+            highest = jnp.max(score, axis=0, keepdims=True)
+            if not fresh:
+                before = state[group : group + 1]
+                highest = jnp.maximum(highest, before)
+                kept = jnp.exp(before - highest)
+            raised = jnp.exp(score - highest)
+            amount = jnp.sum(raised, axis=0, keepdims=True)
+            mixed = jnp.dot(
+                values.astype(narrow), raised.astype(narrow), preferred_element_type=wide
+            )
+            if not fresh:
+                amount = amount + kept * state[group + 2 : group + 3]
+                mixed = mixed + kept * numerator[spots, :]
+            state[group : group + 1] = highest
+            state[group + 2 : group + 3] = amount
+            numerator[spots, :] = mixed
+
+    fold(0, rotary_ref[...], own_places, True, True)
+
+    @pl.when(sp == 1)
+    def _():
+        there = latents.at[1, mine, :]
+        settle(there, cross_sem.at[0])
+        passed = push(there, there, cross_back.at[0], cross_sem.at[3], core_device)
+        settle(rotaries, cross_sem.at[1])
+        passed.wait_recv()
+        fold(1, rotaries[...], pl.ds(0, seq_rows), False, False)
+        passed.wait_send()
+
+    @pl.when(sp == 0)
+    def _():
+        settle(latents.at[0, mine, :], cross_back.at[0])
+        settle(rotary_ref, cross_back.at[1])
+
+    attended = jnp.concatenate(
+        [
+            numerator[:first_width] / state[2:3],
+            numerator[first_width:] / state[3:4],
+        ],
+        axis=0,
+    )
+    attended = attended.T.astype(narrow)
+    loads[1].wait()
+    loads[2].wait()
+
+    def spot(chunk, at, up):
+        return part.at[chunk, at * 2 + up, core]
+
+    def add(chunk, at, up, extra):
+        here = (chunk, at * 2 + up, core)
+        part[here] = (part[here].astype(wide) + extra.astype(wide)).astype(narrow)
+
+    def project(chunk):
+        columns = slice(chunk * width, (chunk + 1) * width)
+        found = jnp.dot(attended, weights[:, columns], preferred_element_type=wide)
+        part[chunk] = found.astype(narrow).reshape(2 * lines, 2, rows, width)
+        push(
+            part.at[chunk, :, 1 - core],
+            core_land.at[chunk],
+            send_sem.at[chunk, 0],
+            core_sem.at[chunk],
+            core_device,
+        )
+
+    def to_side(chunk):
+        settle(core_land.at[chunk], core_sem.at[chunk])
+        for m in range(lines):
+            add(chunk, at_line[m], 1 - row, core_land[chunk, at_line[m] * 2 + 1 - row])
+            push(
+                spot(chunk, at_line[m], 1 - row),
+                side_land.at[chunk, m],
+                send_sem.at[chunk, 1],
+                side_sem.at[chunk, m],
+                y_device,
+            )
+        for m in range(lines):
+            add(chunk, at_line[m], row, core_land[chunk, at_line[m] * 2 + row])
+
+    def to_line(chunk):
+        for m in [*range(1, lines), 0]:
+            settle(side_land.at[chunk, m], side_sem.at[chunk, m])
+            value = part[chunk, at_line[m] * 2 + row, core].astype(wide) + side_land[
+                chunk, m
+            ].astype(wide)
+            if m == 0:
+                total[chunk] = value
+                continue
+            part[chunk, at_line[m] * 2 + row, core] = value.astype(narrow)
+            push(
+                spot(chunk, at_line[m], row),
+                line_land.at[chunk, m - 1],
+                send_sem.at[chunk, 2],
+                line_sem.at[chunk, m - 1],
+                line_device[m],
+            )
+
+    def close(chunk):
+        value = total[chunk]
+        for m in range(1, lines):
+            settle(line_land.at[chunk, m - 1], line_sem.at[chunk, m - 1])
+            value = value + line_land[chunk, m - 1].astype(wide)
+        columns = slice(chunk * width, (chunk + 1) * width)
+        middle_ref[:, columns] = (residual[:, columns].astype(wide) + value).astype(narrow)
+
+    stages = (to_side, to_line, close)
+    loads[3].wait()
+    for step in range(chunks + len(stages)):
+        if step < chunks:
+            project(step)
+        for number, stage in enumerate(stages):
+            chunk = step - 1 - number
+            if 0 <= chunk < chunks:
+                stage(chunk)
+    middle = middle_ref[...].astype(wide)
+    root = lax.rsqrt(jnp.mean(middle * middle, axis=-1, keepdims=True) + norm_epsilon)
+    normed_ref[...] = (middle * root * expert_gain_ref[...]).astype(narrow)
+    for chunk in range(chunks):
+        settle(core_land.at[chunk], send_sem.at[chunk, 0])
+        settle(side_land.at[chunk], send_sem.at[chunk, 1])
+        settle(line_land.at[chunk], send_sem.at[chunk, 2])
+    route_copy.wait_send()
+    settle(codes_ref.at[0], cross_sem.at[2])
+
+
+def run_attention(table, arguments, rows, pitch, chunks, collective_id):
+    (first, second, latent, rotary, _, _, value_first, _, value_second) = arguments[:9]
+    residual = arguments[11]
+    groups, sets = lax.axis_size("sp"), lax.axis_size("tp")
+    lines = sets // 4
+    seq_rows, rank = latent.shape
+    depth = residual.shape[1]
+    width = depth // chunks
+    heads = value_first.shape[0] + value_second.shape[1]
+    narrow, wide = jnp.bfloat16, jnp.float32
+    anywhere = pl.BlockSpec(memory_space=pl.ANY)
+    dma = pltpu.SemaphoreType.DMA
+    specs = [VMEM] * (1 + len(arguments))
+    for place in (2, 9, 10, 11):
+        specs[1 + place] = anywhere
+    return pl.pallas_call(
+        functools.partial(attention_kernel, pitch),
+        out_shape=(
+            jax.ShapeDtypeStruct((rows, depth), narrow),
+            jax.ShapeDtypeStruct((rows, depth), narrow),
+            jax.ShapeDtypeStruct((groups, 8, seq_rows), wide),
+        ),
+        in_specs=specs,
+        out_specs=(VMEM,) * 3,
+        scratch_shapes=[
+            pltpu.VMEM((2, seq_rows, rank), narrow),
+            pltpu.VMEM(rotary.shape, narrow),
+            pltpu.VMEM((first.shape[0] + second.shape[0], seq_rows), narrow),
+            pltpu.VMEM((heads, depth), narrow),
+            pltpu.VMEM((rows, depth), narrow),
+            pltpu.VMEM((8, seq_rows), wide),
+            pltpu.VMEM((heads, seq_rows), wide),
+            pltpu.VMEM((chunks, 2 * lines, 2, rows, width), narrow),
+            pltpu.VMEM((chunks, 2 * lines, rows, width), narrow),
+            pltpu.VMEM((chunks, lines, rows, width), narrow),
+            pltpu.VMEM((chunks, lines - 1, rows, width), narrow),
+            pltpu.VMEM((chunks, rows, width), wide),
+            dma((4,)),
+            dma((4,)),
+            dma((3,)),
+            dma((chunks,)),
+            dma((chunks, lines)),
+            dma((chunks, lines - 1)),
+            dma((chunks, 3)),
+        ],
+        compiler_params=pltpu.CompilerParams(
+            collective_id=collective_id, has_side_effects=True, vmem_limit_bytes=40 << 20
+        ),
+        name="run_attention",
+    )(table, *arguments)
 
 
 def mixture_kernel(
@@ -619,14 +759,15 @@
 
     for tile in range(tiles):
         slots = lax.broadcasted_iota(jnp.int32, (span, tokens), 0)
-        first = slots == code_ref[tile, pl.ds(0, 1), :].astype(jnp.int32)
-        second = slots == code_ref[tile, pl.ds(1, 1), :].astype(jnp.int32)
+        side, place = divmod(tile * tokens, code_ref.shape[2])
+        code = code_ref[side, :, place : place + tokens]
+        slots = slots + sp * span
+        first = slots == code[0:1].astype(jnp.int32)
+        second = slots == code[1:2].astype(jnp.int32)
         chosen = jnp.where(first | second, 1.0, 0.0)
         hot[tile] = chosen.astype(jnp.bfloat16)
         hot_turned[tile] = chosen.T.astype(jnp.bfloat16)
-        portion = jnp.where(first, code_ref[tile, pl.ds(2, 1), :], 0.0) + jnp.where(
-            second, code_ref[tile, pl.ds(3, 1), :], 0.0
-        )
+        portion = jnp.where(first, code[2:3], 0.0) + jnp.where(second, code[3:4], 0.0)
         scale[:, tile * pitch : (tile + 1) * pitch, :] = jnp.sum(
             portion, axis=1, keepdims=True
         ).reshape(experts, pitch, 1)
@@ -809,9 +950,10 @@
     tokens, middle, codes, gate_weight, up_weight, down_weight, pitch, chunks, collective_id
 ):
     experts, depth, units = gate_weight.shape
-    tiles, _, tile_tokens = codes.shape
     rows = tokens.shape[0]
     groups, sets = lax.axis_size("sp"), lax.axis_size("tp")
+    tile_tokens = TILE_TOKENS
+    tiles = groups * sets * rows // tile_tokens
     pairs, lines = groups * sets // 2, sets // 4
     width = depth // chunks
     span = experts * pitch
@@ -860,24 +1002,6 @@
     )(tokens, middle, codes, gate_weight, up_weight, down_weight)
 
 
-def attended_heads(queries, nope, keys, turned, values, allowed, scale):
-    heads = queries.shape[1]
-    wide = keys.reshape(keys.shape[0], heads, nope)
-    shared = jnp.broadcast_to(turned[:, None, :], (turned.shape[0], heads, turned.shape[1]))
-    whole = jnp.concatenate([wide, shared], axis=-1)
-    value_rows = values.reshape(values.shape[0], heads, values.shape[1] // heads)
-    score = jnp.einsum("qhd,khd->hqk", queries, whole, preferred_element_type=jnp.float32) * scale
-    score = jnp.where(allowed, score, masked_score)
-    highest = jnp.max(score, axis=-1, keepdims=True)
-    weights = jnp.exp(score - highest)
-    denominator = jnp.sum(weights, axis=-1)
-    numerator = jnp.einsum(
-        "hqk,khd->hqd", weights.astype(jnp.bfloat16), value_rows, preferred_element_type=jnp.float32
-    )
-    attended = (numerator / denominator[..., None]).astype(jnp.bfloat16)
-    return jnp.swapaxes(attended, 0, 1).reshape(attended.shape[1], -1)
-
-
 def token_body(
     query_first,
     query_second,
@@ -902,63 +1026,36 @@
     sets = lax.axis_size("tp")
     groups = lax.axis_size("sp")
     own_rows = seq_rows // sets
-    local_experts = gate_weight.shape[0]
-    total = groups * seq_rows
-    me = lax.axis_index("sp")
-    core, first, rest, across = cube_steps(groups, sets)
     span_blocks = TILE_TOKENS // own_rows
     pitch = -(-span_blocks * CAP // 16) * 16
-
-    chosen = route_experts.reshape(sets, -1)
-    earlier = jnp.tril(jnp.ones((chosen.shape[1],) * 2, jnp.float32), -1)
-    same = (chosen[:, :, None] == chosen[:, None, :]).astype(jnp.float32)
-    rank = jnp.sum(same * earlier, axis=-1)
-    spot = ((jnp.arange(sets, dtype=jnp.int32) % span_blocks) * CAP).astype(jnp.float32)
-    code = chosen.astype(jnp.float32) * pitch + spot[:, None] + rank
-    code = code.reshape(seq_rows, -1).T
-    scores = route_scores.T
-    raised = jnp.exp(scores - jnp.max(scores, axis=0, keepdims=True))
-    share = raised / jnp.sum(raised, axis=0, keepdims=True)
-    route = jnp.concatenate([code, share, code, share], axis=0)
-
-    rotary = key_rotary.shape[1]
-    wide_rotary = jnp.pad(key_rotary, ((0, 0), (0, -rotary % 128)))
-    latents, turns, routes = exchange(latent, wide_rotary, route, 0)
-
-    places = me * seq_rows + jnp.arange(seq_rows, dtype=jnp.int32)
-    all_places = jnp.arange(total, dtype=jnp.int32)
-    queries_first = turned_queries(query_first, NA, places)
-    queries_second = turned_queries(query_second, NB, places)
-    turned = rotate(
-        turns.reshape(total, -1)[:, :rotary].astype(jnp.float32)[:, None, :], all_places
-    )[:, 0, :].astype(jnp.bfloat16)
-    latent_normed = rms_scaled(latents.reshape(total, -1), latent_gain).astype(jnp.bfloat16)
-    key_first, value_first, key_second, value_second = tuple(
-        jnp.dot(latent_normed, weight, preferred_element_type=jnp.float32).astype(jnp.bfloat16)
-        for weight in (key_up_first, value_up_first, key_up_second, value_up_second)
-    )
-    allowed = (places[:, None] >= all_places[None, :])[None]
-    attended_first = attended_heads(
-        queries_first, NA, key_first, turned, value_first, allowed, (NA + ROPE) ** (-0.5)
-    )
-    attended_second = attended_heads(
-        queries_second, NB, key_second, turned, value_second, allowed, (NB + ROPE) ** (-0.5)
-    )
-    partial = (
-        jnp.dot(attended_first, out_first, preferred_element_type=jnp.float32)
-        + jnp.dot(attended_second, out_second, preferred_element_type=jnp.float32)
-    ).astype(jnp.bfloat16)
-    one, two = tuple(core + first + rest), tuple(core + rest + first)
-    projected = scatter_blocks(partial, (one, two, one, one), sets, sets, 1)
-    own_start = lax.axis_index("tp") * own_rows
-    own_residual = lax.dynamic_slice_in_dim(residual, own_start, own_rows, 0)
-    middle = (own_residual.astype(jnp.float32) + projected).astype(jnp.bfloat16)
-    normed = rms_scaled(middle, expert_gain).astype(jnp.bfloat16)
-    tiles = total // TILE_TOKENS
-    codes = jnp.swapaxes(routes, 0, 1).reshape(8, total)
-    shift = jnp.array([1.0, 1.0, 0.0, 0.0, 1.0, 1.0, 0.0, 0.0], jnp.float32)
-    codes = codes - (shift * (me * local_experts * pitch).astype(jnp.float32))[:, None]
-    codes = jnp.swapaxes(codes.reshape(8, tiles, TILE_TOKENS), 0, 1)
+    half = key_rotary.shape[1] // 2
+    inverse = np.float32(rotary_base) ** (-np.arange(half, dtype=np.float32) / half)
+    angles = inverse[:, None] * np.arange(groups * seq_rows, dtype=np.float32)[None, :]
+    table = np.concatenate([np.cos(angles), np.sin(angles)], axis=0).astype(np.float32)
+    middle, normed, codes = run_attention(
+        jnp.asarray(table),
+        (
+            query_first.T,
+            query_second.T,
+            latent,
+            key_rotary.T,
+            latent_gain[None, :],
+            key_up_first.T,
+            value_up_first.T,
+            key_up_second,
+            value_up_second,
+            out_first,
+            out_second,
+            residual,
+            expert_gain[None, :],
+            route_experts.T,
+            route_scores.T,
+        ),
+        own_rows,
+        pitch,
+        CHUNKS,
+        1,
+    )
     return run_mixture(
         normed, middle, codes, gate_weight, up_weight, down_weight, pitch, CHUNKS, 2
     )

time: 139 us -> 122 us (0.88)
  other arithmetic: 10.7 us -> 0 us
  matrix products: 8.71 us -> 0 us
  local copies, waits for them, and re-layouts: 10.6 us -> 17.8 us
  Pallas kernels: 108 us -> 104 us
    unnamed x35 -> x39, local copies, waits for them, and re-layouts: 7.43 us -> 17.8 us
    pallas_call x2 -> x1, Pallas kernels: 39.9 us -> 31 us  [run_attention(): pl.pallas_call(functools.partial(attention_kernel, pitch), out_shape=(jax...]
    dot_general x8 -> x0, matrix products: 8.71 us -> none  [the longest x2 5.09 us: attended_heads(): jnp.einsum('hqk,khd->hqd', weights.astype(jnp.bfloat16), value_rows, pref...]
    reduce_sum x6 -> x0, other arithmetic: 4.67 us -> none  [the longest x2 2.56 us: rms_scaled(): jnp.mean(wide * wide, axis=-1, keepdims=True) + norm_epsilon]
    pallas_call x1, Pallas kernels: 68.1 us -> 72.5 us  [run_mixture(): pl.pallas_call(functools.partial(mixture_kernel, pitch), out_shape=jax.Sh...]
    convert_element_type x5 -> x0, other arithmetic: 1.85 us -> none  [the longest x1 0.78 us: turned_queries(): shaped[..., nope:].astype(jnp.float32)]
    slice x2 -> x0, local copies, waits for them, and re-layouts: 1.76 us -> none  [turned_queries(): return jnp.concatenate([shaped[..., :nope], turned], axis=-1)]
    transpose x1 -> x0, other arithmetic: 1.43 us -> none  [token_body(): codes = jnp.swapaxes(codes.reshape(8, tiles, TILE_TOKENS), 0, 1)]
where the time goes in v2:
time: 122 us; the launch traced here: 121 us
  Pallas kernels  104 us (85%)
  local copies, waits for them, and re-layouts  17.8 us (15%)
    pallas_call x1, Pallas kernels, run_mixture(): pl.pallas_call(functools.partial(mixture_kernel, pitch), out_shape=jax.Sh...  72.5 us
    pallas_call x1, Pallas kernels, run_attention(): pl.pallas_call(functools.partial(attention_kernel, pitch), out_shape=(jax...  31 us
    unnamed x39, local copies, waits for them, and re-layouts  17.8 us

profile of v2, /device:TPU:0, one launch (start us, length us, event | category | flops | bytes accessed | tf_op | source)
XLA Modules:
  0.0 121.3 jit_solution(7646839540044958352)
XLA Ops:
  0.0 0.0 copy-start
  0.0 1.6 %copy-done = bf16[512,2048]{1,0:T(8,128)(2,1)S(1)} copy-done((bf16[512,2048]{1,0:T(8,128)(2,1)S(1)}, bf16[512,2048]{1,0:T(8,128)(2,1)}, u32[]{:S(2)}) %copy-start) | copy-done | bytes 2097176
  1.6 1.0 copy-done.1
  2.6 1.0 copy-done.2
  3.7 0.9 copy-done.3
  4.6 0.9 copy-done.4
  5.5 0.9 copy-done.7
  6.5 0.9 copy-done.8
  7.4 0.9 copy-done.9
  8.3 0.9 copy-done.10
  9.2 0.8 copy-done.11
  10.0 0.8 copy-done.12
  10.8 0.8 copy-done.13
  11.6 0.7 copy-done.15
  12.3 0.7 copy-done.16
  13.0 0.7 copy-done.17
  13.7 0.7 copy-done.18
  14.3 31.0 %run_attention.1 = (bf16[32,2048]{1,0:T(8,128)(2,1)S(1)}, bf16[32,2048]{1,0:T(8,128)(2,1)S(1)}, f32[2,8,512]{2,1,0:T(8,128)S(1)}) custom-call(f32[32,1024]{1,0:T(8,128)S(1)} %copy-done.9, bf16[96,512]{1,0:T(8,128)(2,1)S(1)} %bitcast.10, bf16[160,512]{1,0:T(8,128)(2,1)S(1)} %bitcast.9, bf16[512,512]{1,0:T(8,128)(2,1)S(1)} %copy-done.1, ...), custom_call_target="tpu_custom_call" | custom-call | tf_op jit(solution)/shard_map/run_attention/pallas_call | solution.py:561
  45.4 0.0 copy-start.5
  45.4 0.6 copy-done.5
  46.0 0.7 copy-done.6
  46.7 0.6 copy-done.14
  47.3 72.5 %run_mixture.1 = bf16[32,2048]{1,0:T(8,128)(2,1)} custom-call(bf16[32,2048]{1,0:T(8,128)(2,1)} %copy-done.6, bf16[32,2048]{1,0:T(8,128)(2,1)} %copy-done.5, f32[2,8,512]{2,1,0:T(8,128)} %copy-done.14, bf16[16,2048,256]{2,1,0:T(8,128)(2,1)} %gate_ref.1, bf16[16,2048,256]{2,1,0:T(8,128)(2,1)} %up_ref.1, bf16[16,256,2048]{2,1,0:T(8,128)(2,1)} %down_ref.1), custom_call_target="tpu_custom_call" | custom-call | tf_op jit(solution)/shard_map/run_mixture/pallas_call | solution.py:963
  119.8 1.6 %copy.21 = bf16[32,2048]{1,0:T(8,128)(2,1)} copy(bf16[32,2048]{1,0:T(8,128)(2,1)} %run_mixture.1) | data formatting | bytes 262144
  (17 shorter events, 0.0 us)
Async XLA Ops:
  0.0 1.6 %copy-start = (bf16[512,2048]{1,0:T(8,128)(2,1)S(1)}, bf16[512,2048]{1,0:T(8,128)(2,1)}, u32[]{:S(2)}) copy-start(bf16[512,2048]{1,0:T(8,128)(2,1)} %residual_ref.1) | copy-start | bytes 6291460
  1.6 1.0 copy-start.1
  2.6 1.0 copy-start.2
  3.7 0.9 copy-start.3
  4.6 0.9 copy-start.4
  5.5 0.9 copy-start.7
  6.4 0.9 copy-start.8
  7.4 0.9 copy-start.9
  8.3 0.9 copy-start.10
  9.2 0.8 copy-start.11
  10.0 0.8 copy-start.12
  10.8 0.8 copy-start.13
  11.6 0.7 copy-start.15
  12.3 0.7 copy-start.16
  13.0 0.7 copy-start.17
  13.7 0.7 copy-start.18
  45.4 0.7 copy-start.5
  46.0 0.7 copy-start.6
  46.7 0.6 copy-start.14

commit v3 on v2

--- a/solution.py
+++ b/solution.py
@@ -225,6 +225,9 @@
 VMEM = pl.BlockSpec(memory_space=pltpu.VMEM)
 TILE_TOKENS = 256
 CHUNKS = 4
+JOINT = 4
+STRIPS = 4
+LAGS = (1, 2, 0)
 
 
 def flipped(value, mask, bits):
@@ -240,19 +243,16 @@
     table_ref,
     first_ref,
     second_ref,
-    latent_ref,
     rotary_ref,
     latent_gain_ref,
     key_first_ref,
     value_first_ref,
     key_second_ref,
     value_second_ref,
-    out_first_ref,
-    out_second_ref,
-    residual_ref,
     expert_gain_ref,
     route_ref,
     score_ref,
+    loads,
     middle_ref,
     normed_ref,
     codes_ref,
@@ -268,7 +268,6 @@
     side_land,
     line_land,
     total,
-    load_sem,
     cross_sem,
     cross_back,
     core_sem,
@@ -279,7 +278,7 @@
     sets = lax.axis_size("tp")
     lines = sets // 4
     bits = lines.bit_length() - 1
-    chunks, _, _, rows, width = part.shape
+    chunks, _, _, _, rows, width = part.shape
     _, seq_rows, rank = latents.shape
     first_nope, second_nope = key_first_ref.shape[0], key_second_ref.shape[1]
     first_width, second_width = value_first_ref.shape[0], value_second_ref.shape[1]
@@ -300,21 +299,6 @@
     for one in everyone:
         pl.semaphore_signal(barrier, inc=1, device_id=one, device_id_type=MESH)
 
-    own_rows = pl.ds(pl.multiple_of(tp * rows, rows), rows)
-    loads = [
-        pltpu.make_async_copy(source, target, load_sem.at[number])
-        for number, (source, target) in enumerate(
-            (
-                (latent_ref, latents.at[0]),
-                (out_first_ref, weights.at[:first_width, :]),
-                (out_second_ref, weights.at[first_width:, :]),
-                (residual_ref.at[own_rows, :], residual),
-            )
-        )
-    ]
-    for copy in loads:
-        copy.start()
-
     def push(source, target, send, receive, where):
         copy = pltpu.make_async_remote_copy(
             src_ref=source,
@@ -331,7 +315,8 @@
         pltpu.make_async_copy(view, view, sem).wait()
 
     mine = pl.ds(pl.multiple_of(core * (seq_rows // 2), seq_rows // 2), seq_rows // 2)
-    loads[0].wait()
+    loads["latent"].wait()
+    loads["rotary"].wait()
     pl.semaphore_wait(barrier, len(everyone))
 
     @pl.when(sp == 0)
@@ -344,6 +329,9 @@
             x_device,
         )
         push(rotary_ref, rotaries, cross_back.at[1], cross_sem.at[1], x_device)
+
+    for name in ("routes", "scores"):
+        loads[name].wait()
 
     tile = 4 * rows
     own_codes = codes_ref.at[sp]
@@ -374,6 +362,17 @@
     own_codes[...] = jnp.concatenate([lists, lists], axis=0)
     route_copy = push(own_codes, own_codes, cross_back.at[2], cross_sem.at[2], x_device)
 
+    for name in (
+        "table",
+        "first",
+        "second",
+        "latent_gain",
+        "key_first",
+        "value_first",
+        "key_second",
+        "value_second",
+    ):
+        loads[name].wait()
     own_places = pl.ds(pl.multiple_of(sp * seq_rows, seq_rows), seq_rows)
 
     def turned(values, where):
@@ -461,54 +460,49 @@
         axis=0,
     )
     attended = attended.T.astype(narrow)
-    loads[1].wait()
-    loads[2].wait()
-
-    def spot(chunk, at, up):
-        return part.at[chunk, at * 2 + up, core]
-
-    def add(chunk, at, up, extra):
-        here = (chunk, at * 2 + up, core)
-        part[here] = (part[here].astype(wide) + extra.astype(wide)).astype(narrow)
+    for name in ("out_first", "out_second", "residual", "expert_gain"):
+        loads[name].wait()
 
     def project(chunk):
         columns = slice(chunk * width, (chunk + 1) * width)
         found = jnp.dot(attended, weights[:, columns], preferred_element_type=wide)
-        part[chunk] = found.astype(narrow).reshape(2 * lines, 2, rows, width)
+        part[chunk] = found.astype(narrow).reshape(lines, 2, 2, rows, width)
         push(
-            part.at[chunk, :, 1 - core],
+            part.at[chunk, :, :, 1 - core],
             core_land.at[chunk],
             send_sem.at[chunk, 0],
             core_sem.at[chunk],
             core_device,
         )
 
+    def add_core(chunk, up):
+        part[chunk, :, up, core] = (
+            part[chunk, :, up, core].astype(wide) + core_land[chunk, :, up].astype(wide)
+        ).astype(narrow)
+
     def to_side(chunk):
         settle(core_land.at[chunk], core_sem.at[chunk])
-        for m in range(lines):
-            add(chunk, at_line[m], 1 - row, core_land[chunk, at_line[m] * 2 + 1 - row])
+        add_core(chunk, 1 - row)
+        push(
+            part.at[chunk, :, 1 - row, core],
+            side_land.at[chunk],
+            send_sem.at[chunk, 1],
+            side_sem.at[chunk],
+            y_device,
+        )
+        add_core(chunk, row)
+
+    def to_line(chunk):
+        settle(side_land.at[chunk], side_sem.at[chunk])
+        total[chunk] = part[chunk, line, row, core].astype(wide) + side_land[chunk, line].astype(
+            wide
+        )
+        part[chunk, :, row, core] = (
+            part[chunk, :, row, core].astype(wide) + side_land[chunk].astype(wide)
+        ).astype(narrow)
+        for m in range(1, lines):
             push(
-                spot(chunk, at_line[m], 1 - row),
-                side_land.at[chunk, m],
-                send_sem.at[chunk, 1],
-                side_sem.at[chunk, m],
-                y_device,
-            )
-        for m in range(lines):
-            add(chunk, at_line[m], row, core_land[chunk, at_line[m] * 2 + row])
-
-    def to_line(chunk):
-        for m in [*range(1, lines), 0]:
-            settle(side_land.at[chunk, m], side_sem.at[chunk, m])
-            value = part[chunk, at_line[m] * 2 + row, core].astype(wide) + side_land[
-                chunk, m
-            ].astype(wide)
-            if m == 0:
-                total[chunk] = value
-                continue
-            part[chunk, at_line[m] * 2 + row, core] = value.astype(narrow)
-            push(
-                spot(chunk, at_line[m], row),
+                part.at[chunk, at_line[m], row, core],
                 line_land.at[chunk, m - 1],
                 send_sem.at[chunk, 2],
                 line_sem.at[chunk, m - 1],
@@ -524,7 +518,6 @@
         middle_ref[:, columns] = (residual[:, columns].astype(wide) + value).astype(narrow)
 
     stages = (to_side, to_line, close)
-    loads[3].wait()
     for step in range(chunks + len(stages)):
         if step < chunks:
             project(step)
@@ -543,65 +536,11 @@
     settle(codes_ref.at[0], cross_sem.at[2])
 
 
-def run_attention(table, arguments, rows, pitch, chunks, collective_id):
-    (first, second, latent, rotary, _, _, value_first, _, value_second) = arguments[:9]
-    residual = arguments[11]
-    groups, sets = lax.axis_size("sp"), lax.axis_size("tp")
-    lines = sets // 4
-    seq_rows, rank = latent.shape
-    depth = residual.shape[1]
-    width = depth // chunks
-    heads = value_first.shape[0] + value_second.shape[1]
-    narrow, wide = jnp.bfloat16, jnp.float32
-    anywhere = pl.BlockSpec(memory_space=pl.ANY)
-    dma = pltpu.SemaphoreType.DMA
-    specs = [VMEM] * (1 + len(arguments))
-    for place in (2, 9, 10, 11):
-        specs[1 + place] = anywhere
-    return pl.pallas_call(
-        functools.partial(attention_kernel, pitch),
-        out_shape=(
-            jax.ShapeDtypeStruct((rows, depth), narrow),
-            jax.ShapeDtypeStruct((rows, depth), narrow),
-            jax.ShapeDtypeStruct((groups, 8, seq_rows), wide),
-        ),
-        in_specs=specs,
-        out_specs=(VMEM,) * 3,
-        scratch_shapes=[
-            pltpu.VMEM((2, seq_rows, rank), narrow),
-            pltpu.VMEM(rotary.shape, narrow),
-            pltpu.VMEM((first.shape[0] + second.shape[0], seq_rows), narrow),
-            pltpu.VMEM((heads, depth), narrow),
-            pltpu.VMEM((rows, depth), narrow),
-            pltpu.VMEM((8, seq_rows), wide),
-            pltpu.VMEM((heads, seq_rows), wide),
-            pltpu.VMEM((chunks, 2 * lines, 2, rows, width), narrow),
-            pltpu.VMEM((chunks, 2 * lines, rows, width), narrow),
-            pltpu.VMEM((chunks, lines, rows, width), narrow),
-            pltpu.VMEM((chunks, lines - 1, rows, width), narrow),
-            pltpu.VMEM((chunks, rows, width), wide),
-            dma((4,)),
-            dma((4,)),
-            dma((3,)),
-            dma((chunks,)),
-            dma((chunks, lines)),
-            dma((chunks, lines - 1)),
-            dma((chunks, 3)),
-        ],
-        compiler_params=pltpu.CompilerParams(
-            collective_id=collective_id, has_side_effects=True, vmem_limit_bytes=40 << 20
-        ),
-        name="run_attention",
-    )(table, *arguments)
-
-
 def mixture_kernel(
     pitch,
+    weight_copies,
     x_ref,
-    middle_ref,
     code_ref,
-    gate_ref,
-    up_ref,
     down_ref,
     out_ref,
     tok,
@@ -630,16 +569,15 @@
     side_back,
     line_back,
     send_back,
-    weight_sem,
     down_sem,
 ):
     groups, sets = lax.axis_size("sp"), lax.axis_size("tp")
     lines = sets // 4
     bits = lines.bit_length() - 1
-    chunks, pairs, _, rows, width = tok.shape
+    chunks, _, _, _, _, rows, width = tok.shape
     experts = picked.shape[0]
     tiles, span, tokens = hot.shape
-    per_tile = tokens // (2 * rows)
+    per_tile = tokens // (4 * rows)
     half = lines // 2
     sp, tp = lax.axis_index("sp"), lax.axis_index("tp")
     core, row, line = tp % 2, (tp // 2) % 2, tp // 4
@@ -647,45 +585,21 @@
     def device(side, at, up, half_chip):
         return {"sp": side, "tp": at * 4 + up * 2 + half_chip}
 
-    def pair_of(side, at, up):
-        return side * (sets // 2) + at * 2 + up
-
     at_line = [flipped(line, m, bits) for m in range(lines)]
-    own = [pair_of(sp, at_line[m], row) for m in range(lines)]
-    by_x = [pair_of(1 - sp, at_line[m], row) for m in range(lines)]
-    by_y = [pair_of(sp, at_line[m], 1 - row) for m in range(lines)]
-    by_xy = [pair_of(1 - sp, at_line[m], 1 - row) for m in range(lines)]
+    high = line // half
+    near = pl.ds(high * half, half)
+    far = pl.ds((1 - high) * half, half)
+    whole = slice(None)
     x_device = device(1 - sp, line, row, core)
     y_device = device(sp, line, 1 - row, core)
     core_device = device(sp, line, row, 1 - core)
     line_device = [device(sp, at_line[m], row, core) for m in range(lines)]
 
-    barrier = pltpu.get_barrier_semaphore()
-    everyone = [x_device, y_device, core_device] + line_device[1:]
-    for one in everyone:
-        pl.semaphore_signal(barrier, inc=1, device_id=one, device_id_type=MESH)
-
-    def weight_copies(chunk):
-        part = pl.ds(chunk * width, width)
-        slot = chunk % 2
-        return (
-            pltpu.make_async_copy(
-                gate_ref.at[:, part, :], gate_buf.at[slot], weight_sem.at[slot, 0]
-            ),
-            pltpu.make_async_copy(up_ref.at[:, part, :], up_buf.at[slot], weight_sem.at[slot, 1]),
-        )
-
     def down_copy(chunk):
         part = pl.ds(chunk * width, width)
         return pltpu.make_async_copy(
             down_ref.at[:, :, part], down_buf.at[chunk], down_sem.at[chunk]
         )
-
-    for chunk in range(min(2, chunks)):
-        for copy in weight_copies(chunk):
-            copy.start()
-
-    pl.semaphore_wait(barrier, len(everyone))
 
     def push(source, target, send, receive, where):
         pltpu.make_async_remote_copy(
@@ -700,62 +614,63 @@
     def settle(view, sem):
         pltpu.make_async_copy(view, view, sem).wait()
 
-    def spot(chunk, pair):
-        return tok.at[chunk, pair, core]
-
-    def share(chunk, pair, part):
-        push(
-            spot(chunk, pair),
-            spot(chunk, pair),
-            pass_sem.at[chunk, part],
-            core_sem.at[chunk],
-            core_device,
-        )
+    def share(chunk, side, up, number):
+        column = tok.at[chunk, side, :, up, core]
+        push(column, column, pass_sem.at[chunk, 3], core_sem.at[chunk, number], core_device)
 
     def send_own(chunk):
         source = x_ref.at[:, pl.ds(chunk * width, width)]
-        target = spot(chunk, own[0])
-        early = pass_sem.at[chunk, 0]
+        target = tok.at[chunk, sp, line, row, core]
         for m in range(1, lines):
-            push(source, target, early, line_sem.at[chunk, m - 1], line_device[m])
-        push(source, target, early, side_sem.at[chunk, 0, 0], x_device)
-        push(source, target, early, side_sem.at[chunk, 1, 0], y_device)
-        push(source, target, early, core_sem.at[chunk], core_device)
+            push(source, target, pass_sem.at[chunk, 2], line_sem.at[chunk, m - 1], line_device[m])
+        push(source, target, pass_sem.at[chunk, 0], side_sem.at[chunk, 0, 0], x_device)
+        push(source, target, pass_sem.at[chunk, 0], side_sem.at[chunk, 1, 0], y_device)
 
     def pass_line(chunk):
+        def onward(here, number):
+            early = pass_sem.at[chunk, 0]
+            push(here, here, early, side_sem.at[chunk, 0, number], x_device)
+            push(here, here, early, side_sem.at[chunk, 1, number], y_device)
+
         for m in range(1, lines):
-            settle(spot(chunk, own[m]), line_sem.at[chunk, m - 1])
-            here = spot(chunk, own[m])
-            early = pass_sem.at[chunk, 0]
-            push(here, here, early, side_sem.at[chunk, 0, m], x_device)
-            push(here, here, early, side_sem.at[chunk, 1, m], y_device)
-            share(chunk, own[m], 0)
+            here = tok.at[chunk, sp, at_line[m], row, core]
+            settle(here, line_sem.at[chunk, m - 1])
+            if m < half:
+                onward(here, m)
+        onward(tok.at[chunk, sp, far, row, core], half)
+        share(chunk, sp, row, 0)
+
+    def settle_near(chunk, axis, side, up):
+        for m in range(half):
+            settle(tok.at[chunk, side, at_line[m], up, core], side_sem.at[chunk, axis, m])
 
     def pass_side(chunk):
-        for m in [*range(half, lines), *range(half)]:
-            turn = ((0, by_x), (1, by_y)) if m >= half else ((1, by_y), (0, by_x))
-            for axis, column in turn:
-                here = spot(chunk, column[m])
-                settle(here, side_sem.at[chunk, axis, m])
-                late = pass_sem.at[chunk, 1]
-                if axis == 0 and m >= half:
-                    push(here, here, late, diag_sem.at[chunk, m], y_device)
-                if axis == 1 and m < half:
-                    push(here, here, late, diag_sem.at[chunk, m], x_device)
-                share(chunk, column[m], 1)
+        by_x, by_y = (chunk, 1 - sp), (chunk, sp)
+        late = pass_sem.at[chunk, 1]
+        settle_near(chunk, 1, sp, 1 - row)
+        here = tok.at[(*by_y, near, 1 - row, core)]
+        push(here, here, late, diag_sem.at[chunk, 1], x_device)
+        here = tok.at[(*by_x, far, row, core)]
+        settle(here, side_sem.at[chunk, 0, half])
+        push(here, here, late, diag_sem.at[chunk, 0], y_device)
+        settle_near(chunk, 0, 1 - sp, row)
+        share(chunk, 1 - sp, row, 1)
+        settle(tok.at[(*by_y, far, 1 - row, core)], side_sem.at[chunk, 1, half])
+        share(chunk, sp, 1 - row, 2)
 
     def pass_diag(chunk):
-        for m in range(lines):
-            settle(spot(chunk, by_xy[m]), diag_sem.at[chunk, m])
-            share(chunk, by_xy[m], 1)
+        for number, part in enumerate((far, near)):
+            settle(tok.at[chunk, 1 - sp, part, 1 - row, core], diag_sem.at[chunk, number])
+        share(chunk, 1 - sp, 1 - row, 3)
 
     def finish(chunk):
-        settle(tok.at[chunk, :, 0], core_sem.at[chunk])
+        for number in range(4):
+            settle(tok.at[chunk, 0, :, 0, 0], core_sem.at[chunk, number])
 
     for chunk in range(chunks):
         send_own(chunk)
     for chunk in range(chunks):
-        tok[chunk, own[0], core] = x_ref[:, chunk * width : (chunk + 1) * width]
+        tok[chunk, sp, line, row, core] = x_ref[:, chunk * width : (chunk + 1) * width]
 
     for tile in range(tiles):
         slots = lax.broadcasted_iota(jnp.int32, (span, tokens), 0)
@@ -772,24 +687,31 @@
             portion, axis=1, keepdims=True
         ).reshape(experts, pitch, 1)
 
-    def pick(chunk, tile):
-        block = tok[chunk, tile * per_tile : (tile + 1) * per_tile].reshape(tokens, width)
-        found = jnp.dot(hot[tile], block, preferred_element_type=jnp.float32)
-        picked[:, tile * pitch : (tile + 1) * pitch, :] = found.astype(jnp.bfloat16).reshape(
-            experts, pitch, width
-        )
-
-    def hidden(chunk, low, high):
-        slot = chunk % 2
+    joined = picked.shape[2] // width
+    steps = chunks // joined
+
+    def pick(chunk):
+        finish(chunk)
+        place = chunk % joined * width
+        for tile in range(tiles):
+            side, start = divmod(tile * per_tile, lines)
+            block = tok[chunk, side, start : start + per_tile].reshape(tokens, width)
+            found = jnp.dot(hot[tile], block, preferred_element_type=jnp.float32)
+            picked[:, tile * pitch : (tile + 1) * pitch, place : place + width] = found.astype(
+                jnp.bfloat16
+            ).reshape(experts, pitch, width)
+
+    def hidden(step, low, high):
+        slot = step % 2
 
         def one(expert, carry):
             block = picked[expert]
             gate = jnp.dot(block, gate_buf[slot, expert], preferred_element_type=jnp.float32)
             upward = jnp.dot(block, up_buf[slot, expert], preferred_element_type=jnp.float32)
-            if chunk > 0:
+            if step > 0:
                 gate = gate + gate_sum[expert]
                 upward = upward + up_sum[expert]
-            if chunk + 1 < chunks:
+            if step + 1 < steps:
                 gate_sum[expert] = gate
                 up_sum[expert] = upward
             else:
@@ -798,37 +720,40 @@
 
         lax.fori_loop(low, high, one, 0, unroll=2)
 
-    pass_line(0)
-    if chunks > 1:
-        pass_line(1)
-    pass_side(0)
-    if chunks > 2:
-        pass_line(2)
-    pass_diag(0)
-    for chunk in range(chunks):
-        finish(chunk)
-        for tile in range(tiles):
-            pick(chunk, tile)
-        if chunk + 1 < chunks:
-            pass_side(chunk + 1)
-        for copy in weight_copies(chunk):
+    clock = [0]
+
+    def tick():
+        now = clock[0]
+        clock[0] = now + 1
+        for stage, lag in ((pass_line, 0), (pass_side, LAGS[0]), (pass_diag, LAGS[1])):
+            if 0 <= now - lag < chunks:
+                stage(now - lag)
+
+    def reach(chunk):
+        while clock[0] <= min(chunk + LAGS[2], chunks - 1) + LAGS[1]:
+            tick()
+
+    for step in range(steps):
+        for number in range(joined):
+            reach(step * joined + number)
+            pick(step * joined + number)
+        for copy in weight_copies(step):
             copy.wait()
-        hidden(chunk, 0, experts // 2)
-        if chunk + 3 < chunks:
-            pass_line(chunk + 3)
-        if chunk + 1 < chunks:
-            pass_diag(chunk + 1)
-        hidden(chunk, experts // 2, experts)
-        if chunk + 2 < chunks:
-            for copy in weight_copies(chunk + 2):
+        hidden(step, 0, experts // 2)
+        reach((step + 1) * joined)
+        hidden(step, experts // 2, experts)
+        if step + 2 < steps:
+            for copy in weight_copies(step + 2):
                 copy.start()
-        if chunk == 0:
+        if step == 0:
             for later in range(chunks):
                 down_copy(later).start()
 
     for chunk in range(chunks):
-        settle(tok.at[chunk, : pairs - 1, 0], pass_sem.at[chunk, 0])
-        settle(tok.at[chunk, :, 0], pass_sem.at[chunk, 1])
+        settle(core_land.at[chunk, 0], pass_sem.at[chunk, 0])
+        settle(diag_land.at[chunk], pass_sem.at[chunk, 1])
+        settle(line_land.at[chunk], pass_sem.at[chunk, 2])
+        settle(core_land.at[chunk], pass_sem.at[chunk, 3])
 
     def lower(chunk):
         down_copy(chunk).wait()
@@ -837,85 +762,93 @@
             result = jnp.dot(
                 active[expert], down_buf[chunk, expert], preferred_element_type=jnp.float32
             )
-            picked[expert] = (result * scale[expert]).astype(jnp.bfloat16)
+            picked[expert, :, :width] = (result * scale[expert]).astype(jnp.bfloat16)
             return carry
 
         lax.fori_loop(0, experts, one, 0, unroll=2)
         for tile in range(tiles):
-            block = picked[:, tile * pitch : (tile + 1) * pitch, :].reshape(span, width)
+            block = picked[:, tile * pitch : (tile + 1) * pitch, :width].reshape(span, width)
             total = jnp.dot(hot_turned[tile], block, preferred_element_type=jnp.float32)
-            tok[chunk, tile * per_tile : (tile + 1) * per_tile] = total.astype(
-                jnp.bfloat16
-            ).reshape(per_tile, 2, rows, width)
+            side, start = divmod(tile * per_tile, lines)
+            tok[chunk, side, start : start + per_tile] = total.astype(jnp.bfloat16).reshape(
+                per_tile, 2, 2, rows, width
+            )
 
     def meet_core(chunk):
         push(
-            tok.at[chunk, :, 1 - core],
+            tok.at[chunk, :, :, :, 1 - core],
             core_land.at[chunk],
             send_back.at[chunk, 0],
             core_back.at[chunk],
             core_device,
         )
 
-    def add_core(chunk, pair):
-        tok[chunk, pair, core] = (
-            tok[chunk, pair, core].astype(jnp.float32) + core_land[chunk, pair].astype(jnp.float32)
-        ).astype(jnp.bfloat16)
+    def add(chunk, side, part, up, extra):
+        here = (chunk, side, part, up, core)
+        tok[here] = (tok[here].astype(jnp.float32) + extra.astype(jnp.float32)).astype(jnp.bfloat16)
+
+    def add_core(chunk, side, part, up):
+        add(chunk, side, part, up, core_land[chunk, side, part, up])
 
     def back_diag(chunk):
         settle(core_land.at[chunk], core_back.at[chunk])
         send = send_back.at[chunk, 1]
-        for m in range(lines):
-            add_core(chunk, by_xy[m])
+        for number, (part, where) in enumerate(((far, y_device), (near, x_device))):
+            add_core(chunk, 1 - sp, part, 1 - row)
             push(
-                spot(chunk, by_xy[m]),
-                diag_land.at[chunk, m],
+                tok.at[chunk, 1 - sp, part, 1 - row, core],
+                diag_land.at[chunk, part],
                 send,
-                diag_back.at[chunk, m],
-                y_device if m >= half else x_device,
-            )
-        for m in range(lines):
-            axis, column, where = (1, by_y, y_device) if m >= half else (0, by_x, x_device)
-            add_core(chunk, column[m])
-            push(
-                spot(chunk, column[m]),
-                side_land.at[chunk, axis, m],
-                send,
-                side_back.at[chunk, axis, m],
+                diag_back.at[chunk, number],
                 where,
             )
-        for m in range(lines):
-            add_core(chunk, (by_x if m >= half else by_y)[m])
-            add_core(chunk, own[m])
-
-    def back_side(chunk):
-        for m in range(lines):
-            axis, column, where = (0, by_x, x_device) if m >= half else (1, by_y, y_device)
-            settle(diag_land.at[chunk, m], diag_back.at[chunk, m])
-            tok[chunk, column[m], core] = (
-                tok[chunk, column[m], core].astype(jnp.float32)
-                + diag_land[chunk, m].astype(jnp.float32)
-            ).astype(jnp.bfloat16)
+        for axis, (part, side, up, where) in enumerate(
+            ((near, 1 - sp, row, x_device), (far, sp, 1 - row, y_device))
+        ):
+            add_core(chunk, side, part, up)
             push(
-                spot(chunk, column[m]),
-                side_land.at[chunk, axis, m],
-                send_back.at[chunk, 2],
-                side_back.at[chunk, axis, m],
+                tok.at[chunk, side, part, up, core],
+                side_land.at[chunk, axis, part],
+                send,
+                side_back.at[chunk, axis, 0],
                 where,
             )
+        add_core(chunk, 1 - sp, far, row)
+        add_core(chunk, sp, near, 1 - row)
+        add_core(chunk, sp, whole, row)
+
+    def back_side(chunk):
+        for axis, (part, side, up, where) in enumerate(
+            ((far, 1 - sp, row, x_device), (near, sp, 1 - row, y_device))
+        ):
+            settle(diag_land.at[chunk, part], diag_back.at[chunk, axis])
+            add(chunk, side, part, up, diag_land[chunk, part])
+            push(
+                tok.at[chunk, side, part, up, core],
+                side_land.at[chunk, axis, part],
+                send_back.at[chunk, 2],
+                side_back.at[chunk, axis, 1],
+                where,
+            )
 
     def back_line(chunk):
-        for m in [*range(1, lines), 0]:
-            total = tok[chunk, own[m], core].astype(jnp.float32)
-            for axis in range(2):
-                settle(side_land.at[chunk, axis, m], side_back.at[chunk, axis, m])
-                total = total + side_land[chunk, axis, m].astype(jnp.float32)
-            if m == 0:
-                own_sum[chunk] = total
-                continue
-            tok[chunk, own[m], core] = total.astype(jnp.bfloat16)
+        for axis in range(2):
+            for number in range(2):
+                settle(side_land.at[chunk, axis, :half], side_back.at[chunk, axis, number])
+        own_sum[chunk] = tok[chunk, sp, line, row, core].astype(jnp.float32) + (
+            side_land[chunk, 0, line].astype(jnp.float32)
+            + side_land[chunk, 1, line].astype(jnp.float32)
+        )
+        add(
+            chunk,
+            sp,
+            whole,
+            row,
+            side_land[chunk, 0].astype(jnp.float32) + side_land[chunk, 1].astype(jnp.float32),
+        )
+        for m in range(1, lines):
             push(
-                spot(chunk, own[m]),
+                tok.at[chunk, sp, at_line[m], row, core],
                 line_land.at[chunk, m - 1],
                 send_back.at[chunk, 3],
                 line_back.at[chunk, m - 1],
@@ -928,7 +861,7 @@
             settle(line_land.at[chunk, m - 1], line_back.at[chunk, m - 1])
             total = total + line_land[chunk, m - 1].astype(jnp.float32)
         part = slice(chunk * width, (chunk + 1) * width)
-        out_ref[:, part] = (middle_ref[:, part].astype(jnp.float32) + total).astype(jnp.bfloat16)
+        out_ref[:, part] = total
 
     stages = (back_diag, back_side, back_line, close)
     for step in range(chunks + len(stages)):
@@ -941,65 +874,203 @@
                 stage(chunk)
     for chunk in range(chunks):
         settle(core_land.at[chunk], send_back.at[chunk, 0])
-        settle(tok.at[chunk, : 2 * lines, 0], send_back.at[chunk, 1])
-        settle(tok.at[chunk, :lines, 0], send_back.at[chunk, 2])
-        settle(tok.at[chunk, : lines - 1, 0], send_back.at[chunk, 3])
-
-
-def run_mixture(
-    tokens, middle, codes, gate_weight, up_weight, down_weight, pitch, chunks, collective_id
-):
+        settle(core_land.at[chunk, 0], send_back.at[chunk, 1])
+        settle(diag_land.at[chunk], send_back.at[chunk, 2])
+        settle(line_land.at[chunk], send_back.at[chunk, 3])
+
+
+def layer_kernel(pitch, names, attention_count, *refs):
+    table = dict(zip(names, refs))
+    refs = refs[len(names) :]
+    gate_ref, up_ref, down_ref, out_ref, middle_ref = refs[:5]
+    refs = refs[5:]
+    normed, codes, latents, weights, residual = refs[:5]
+    refs = refs[5:]
+    held = [name for name in names if name not in PLACED]
+    inputs = dict(zip(held, refs))
+    refs = refs[len(held) :]
+    load_sem, gate_buf, up_buf, weight_sem = refs[:4]
+    refs = refs[4:]
+    attention_refs, mixture_refs = refs[:attention_count], refs[attention_count:]
+    rows = normed.shape[0]
+    first_width = table["out_first"].shape[0]
+    own_rows = pl.ds(pl.multiple_of(lax.axis_index("tp") * rows, rows), rows)
+    width = gate_buf.shape[2]
+
+    def load(number, name):
+        source = table[name]
+        if name == "latent":
+            target = latents.at[0]
+        elif name == "out_first":
+            target = weights.at[:first_width, :]
+        elif name == "out_second":
+            target = weights.at[first_width:, :]
+        elif name == "residual":
+            source, target = source.at[own_rows, :], residual
+        else:
+            target = inputs[name]
+        return pltpu.make_async_copy(source, target, load_sem.at[number])
+
+    loads = {name: load(number, name) for number, name in enumerate(names)}
+
+    def weight_copies(step):
+        part = pl.ds(step * width, width)
+        slot = step % 2
+        return (
+            pltpu.make_async_copy(
+                gate_ref.at[:, part, :], gate_buf.at[slot], weight_sem.at[slot, 0]
+            ),
+            pltpu.make_async_copy(up_ref.at[:, part, :], up_buf.at[slot], weight_sem.at[slot, 1]),
+        )
+
+    for copy in loads.values():
+        copy.start()
+    for step in range(2):
+        for copy in weight_copies(step):
+            copy.start()
+    ready = [inputs[name] for name in held]
+    (rotaries, queries, state, numerator, *rest) = attention_refs
+    attention_kernel(
+        pitch,
+        *ready,
+        loads,
+        middle_ref,
+        normed,
+        codes,
+        latents,
+        rotaries,
+        queries,
+        weights,
+        residual,
+        state,
+        numerator,
+        *rest,
+    )
+    tok, hot, hot_turned, scale, picked, gate_sum, up_sum, active, *more = mixture_refs
+    mixture_kernel(
+        pitch,
+        weight_copies,
+        normed,
+        codes,
+        down_ref,
+        out_ref,
+        tok,
+        hot,
+        hot_turned,
+        scale,
+        picked,
+        gate_sum,
+        up_sum,
+        active,
+        gate_buf,
+        up_buf,
+        *more,
+    )
+
+
+PLACED = ("latent", "out_first", "out_second", "residual")
+HELD = (
+    "table",
+    "first",
+    "second",
+    "rotary",
+    "latent_gain",
+    "key_first",
+    "value_first",
+    "key_second",
+    "value_second",
+    "expert_gain",
+    "routes",
+    "scores",
+)
+
+
+def run_layer(named, gate_weight, up_weight, down_weight, rows, pitch, collective_id):
+    groups, sets = lax.axis_size("sp"), lax.axis_size("tp")
+    lines = sets // 4
+    seq_rows, rank = named["latent"].shape
     experts, depth, units = gate_weight.shape
-    rows = tokens.shape[0]
-    groups, sets = lax.axis_size("sp"), lax.axis_size("tp")
-    tile_tokens = TILE_TOKENS
-    tiles = groups * sets * rows // tile_tokens
-    pairs, lines = groups * sets // 2, sets // 4
-    width = depth // chunks
+    width, joint = depth // CHUNKS, depth // JOINT
+    strip = depth // STRIPS
+    first, second, rotary = named["first"], named["second"], named["rotary"]
+    heads = named["out_first"].shape[0] + named["out_second"].shape[0]
+    tiles = groups * sets * rows // TILE_TOKENS
     span = experts * pitch
+    slots = tiles * pitch
     narrow, wide = jnp.bfloat16, jnp.float32
     anywhere = pl.BlockSpec(memory_space=pl.ANY)
-    dma = pltpu.SemaphoreType.DMA
+    dma, keep = pltpu.SemaphoreType.DMA, pltpu.VMEM
+    attention = [
+        keep(rotary.shape, narrow),
+        keep((first.shape[0] + second.shape[0], seq_rows), narrow),
+        keep((8, seq_rows), wide),
+        keep((heads, seq_rows), wide),
+        keep((STRIPS, lines, 2, 2, rows, strip), narrow),
+        keep((STRIPS, lines, 2, rows, strip), narrow),
+        keep((STRIPS, lines, rows, strip), narrow),
+        keep((STRIPS, lines - 1, rows, strip), narrow),
+        keep((STRIPS, rows, strip), wide),
+        dma((4,)),
+        dma((3,)),
+        dma((STRIPS,)),
+        dma((STRIPS,)),
+        dma((STRIPS, lines - 1)),
+        dma((STRIPS, 3)),
+    ]
+    mixture = [
+        keep((CHUNKS, groups, lines, 2, 2, rows, width), narrow),
+        keep((tiles, span, TILE_TOKENS), narrow),
+        keep((tiles, TILE_TOKENS, span), narrow),
+        keep((experts, slots, 1), wide),
+        keep((experts, slots, joint), narrow),
+        keep((experts, slots, units), wide),
+        keep((experts, slots, units), wide),
+        keep((experts, slots, units), narrow),
+        keep((CHUNKS, experts, units, width), narrow),
+        keep((CHUNKS, groups, lines, 2, rows, width), narrow),
+        keep((CHUNKS, lines, rows, width), narrow),
+        keep((CHUNKS, 2, lines, rows, width), narrow),
+        keep((CHUNKS, lines - 1, rows, width), narrow),
+        keep((CHUNKS, rows, width), wide),
+        dma((CHUNKS, lines - 1)),
+        dma((CHUNKS, 2, lines // 2 + 1)),
+        dma((CHUNKS, 2)),
+        dma((CHUNKS, 4)),
+        dma((CHUNKS, 4)),
+        dma((CHUNKS,)),
+        dma((CHUNKS, 2)),
+        dma((CHUNKS, 2, 2)),
+        dma((CHUNKS, lines - 1)),
+        dma((CHUNKS, 4)),
+        dma((CHUNKS,)),
+    ]
+    names = HELD + PLACED
+    shared = [
+        keep((rows, depth), narrow),
+        keep((groups, 8, seq_rows), wide),
+        keep((2, seq_rows, rank), narrow),
+        keep((heads, depth), narrow),
+        keep((rows, depth), narrow),
+        *[keep(named[name].shape, named[name].dtype) for name in HELD],
+        dma((len(names),)),
+        keep((2, experts, joint, units), narrow),
+        keep((2, experts, joint, units), narrow),
+        dma((2, 2)),
+    ]
     return pl.pallas_call(
-        functools.partial(mixture_kernel, pitch),
-        out_shape=jax.ShapeDtypeStruct(tokens.shape, jnp.bfloat16),
-        in_specs=[VMEM, VMEM, VMEM, anywhere, anywhere, anywhere],
-        out_specs=VMEM,
-        scratch_shapes=[
-            pltpu.VMEM((chunks, pairs, 2, rows, width), narrow),
-            pltpu.VMEM((tiles, span, tile_tokens), narrow),
-            pltpu.VMEM((tiles, tile_tokens, span), narrow),
-            pltpu.VMEM((experts, tiles * pitch, 1), wide),
-            pltpu.VMEM((experts, tiles * pitch, width), narrow),
-            pltpu.VMEM((experts, tiles * pitch, units), wide),
-            pltpu.VMEM((experts, tiles * pitch, units), wide),
-            pltpu.VMEM((experts, tiles * pitch, units), narrow),
-            pltpu.VMEM((2, experts, width, units), narrow),
-            pltpu.VMEM((2, experts, width, units), narrow),
-            pltpu.VMEM((chunks, experts, units, width), narrow),
-            pltpu.VMEM((chunks, pairs, rows, width), narrow),
-            pltpu.VMEM((chunks, lines, rows, width), narrow),
-            pltpu.VMEM((chunks, 2, lines, rows, width), narrow),
-            pltpu.VMEM((chunks, lines - 1, rows, width), narrow),
-            pltpu.VMEM((chunks, rows, width), wide),
-            dma((chunks, lines - 1)),
-            dma((chunks, 2, lines)),
-            dma((chunks, lines)),
-            dma((chunks,)),
-            dma((chunks, 2)),
-            dma((chunks,)),
-            dma((chunks, lines)),
-            dma((chunks, 2, lines)),
-            dma((chunks, lines - 1)),
-            dma((chunks, 4)),
-            dma((2, 2)),
-            dma((chunks,)),
-        ],
+        functools.partial(layer_kernel, pitch, names, len(attention)),
+        out_shape=(
+            jax.ShapeDtypeStruct((rows, depth), wide),
+            jax.ShapeDtypeStruct((rows, depth), narrow),
+        ),
+        in_specs=[anywhere] * (len(names) + 3),
+        out_specs=(VMEM, VMEM),
+        scratch_shapes=shared + attention + mixture,
         compiler_params=pltpu.CompilerParams(
             collective_id=collective_id, has_side_effects=True, vmem_limit_bytes=63 << 20
         ),
-        name="run_mixture",
-    )(tokens, middle, codes, gate_weight, up_weight, down_weight)
+        name="run_layer",
+    )(*[named[name] for name in names], gate_weight, up_weight, down_weight)
 
 
 def token_body(
@@ -1032,33 +1103,28 @@
     inverse = np.float32(rotary_base) ** (-np.arange(half, dtype=np.float32) / half)
     angles = inverse[:, None] * np.arange(groups * seq_rows, dtype=np.float32)[None, :]
     table = np.concatenate([np.cos(angles), np.sin(angles)], axis=0).astype(np.float32)
-    middle, normed, codes = run_attention(
-        jnp.asarray(table),
-        (
-            query_first.T,
-            query_second.T,
-            latent,
-            key_rotary.T,
-            latent_gain[None, :],
-            key_up_first.T,
-            value_up_first.T,
-            key_up_second,
-            value_up_second,
-            out_first,
-            out_second,
-            residual,
-            expert_gain[None, :],
-            route_experts.T,
-            route_scores.T,
-        ),
-        own_rows,
-        pitch,
-        CHUNKS,
-        1,
-    )
-    return run_mixture(
-        normed, middle, codes, gate_weight, up_weight, down_weight, pitch, CHUNKS, 2
-    )
+    named = {
+        "table": jnp.asarray(table),
+        "first": query_first.T,
+        "second": query_second.T,
+        "latent": latent,
+        "rotary": key_rotary.T,
+        "latent_gain": latent_gain[None, :],
+        "key_first": key_up_first.T,
+        "value_first": value_up_first.T,
+        "key_second": key_up_second,
+        "value_second": value_up_second,
+        "out_first": out_first,
+        "out_second": out_second,
+        "residual": residual,
+        "expert_gain": expert_gain[None, :],
+        "routes": route_experts.T,
+        "scores": route_scores.T,
+    }
+    mixture, middle = run_layer(
+        named, gate_weight, up_weight, down_weight, own_rows, pitch, 0
+    )
+    return (middle.astype(jnp.float32) + mixture).astype(jnp.bfloat16)
 
 
 def solution(mesh):

time: 122 us -> 102 us (0.84)
  local copies, waits for them, and re-layouts: 17.8 us -> 0 us
  Pallas kernels: 104 us -> 100 us
  other arithmetic: 0 us -> 1.66 us
    unnamed x39 -> x0, local copies, waits for them, and re-layouts: 17.8 us -> none
    pallas_call x2 -> x1, Pallas kernels: 104 us -> 100 us  [run_layer(): pl.pallas_call(functools.partial(layer_kernel, pitch, names, len(attentio...]
    convert_element_type x0 -> x1, other arithmetic: none -> 1.66 us  [token_body(): return (middle.astype(jnp.float32) + mixture).astype(jnp.bfloat16)]
where the time goes in v3:
time: 102 us
  Pallas kernels  100 us (98%)
  other arithmetic  1.66 us (2%)
    pallas_call x1, Pallas kernels, run_layer(): pl.pallas_call(functools.partial(layer_kernel, pitch, names, len(attentio...  100 us

profile of v3, /device:TPU:0, one launch (start us, length us, event | category | flops | bytes accessed | tf_op | source)
XLA Modules:
  0.0 101.8 jit_solution(5942699647386720236)
XLA Ops:
  0.0 100.1 %run_layer.1 = (f32[32,2048]{1,0:T(8,128)}, bf16[32,2048]{1,0:T(8,128)(2,1)}) custom-call(f32[32,1024]{1,0:T(8,128)} %constant.2.clone.refs_0_, bf16[96,512]{1,0:T(8,128)(2,1)} %bitcast.10, bf16[160,512]{1,0:T(8,128)(2,1)} %bitcast.9, bf16[32,512]{1,0:T(8,128)(2,1)} %bitcast.13, f32[1,512]{1,0:T(1,128)} %bitcast.17, bf16[64,512]{1,0:T(8,128)(2,1)} %bitcast.11, ...), custom_call_target="tpu_custom_call" | custom-call | tf_op jit(solution)/shard_map/run_layer/pallas_call | solution.py:1060
  100.2 1.7 %add_convert_fusion = bf16[32,2048]{1,0:T(8,128)(2,1)} fusion(f32[32,2048]{1,0:T(8,128)} %get-tuple-element.8, bf16[32,2048]{1,0:T(8,128)(2,1)} %get-tuple-element.7), kind=kLoop, calls=%fused_computation | loop fusion | flops 196608 | bytes 524288 | tf_op jit(solution)/shard_map/convert_element_type | solution.py:1127

commit v4 on v3

--- a/solution.py
+++ b/solution.py
@@ -227,7 +227,12 @@
 CHUNKS = 4
 JOINT = 4
 STRIPS = 4
-LAGS = (1, 2, 0)
+EARLY = 2
+ORDER = (
+    "L0", "O2", "L1", "S0", "O3", "L2", "D0", "S1", "P0", "L3", "A0", "D1", "S2", "B0", "P1",
+    "A1", "D2", "S3", "B1", "P2", "A2", "D3", "B2", "P3", "A3", "B3",
+)
+PIECES = 2
 
 
 def flipped(value, mask, bits):
@@ -314,21 +319,28 @@
     def settle(view, sem):
         pltpu.make_async_copy(view, view, sem).wait()
 
+    some = seq_rows // (2 * PIECES)
     mine = pl.ds(pl.multiple_of(core * (seq_rows // 2), seq_rows // 2), seq_rows // 2)
+
+    def piece(side, number):
+        return pl.ds(pl.multiple_of((side * PIECES + number) * some, some), some)
+
     loads["latent"].wait()
     loads["rotary"].wait()
     pl.semaphore_wait(barrier, len(everyone))
 
     @pl.when(sp == 0)
     def _():
-        push(
-            latents.at[0, mine, :],
-            latents.at[1, mine, :],
-            cross_back.at[0],
-            cross_sem.at[0],
-            x_device,
-        )
         push(rotary_ref, rotaries, cross_back.at[1], cross_sem.at[1], x_device)
+        for number in range(PIECES):
+            here = piece(core, number)
+            push(
+                latents.at[0, here, :],
+                latents.at[1, here, :],
+                cross_back.at[0],
+                cross_sem.at[3 + number],
+                x_device,
+            )
 
     for name in ("routes", "scores"):
         loads[name].wait()
@@ -390,8 +402,8 @@
     value_second = value_second_ref[...].astype(wide).T.astype(narrow)
     across = (((1,), (1,)), ((), ()))
 
-    def fold(slot, rotary_values, where, causal, fresh):
-        raw = latents[slot].astype(wide)
+    def fold(slot, span, rotary_values, where, causal, fresh):
+        raw = latents[slot, span, :].astype(wide)
         root = lax.rsqrt(jnp.mean(raw * raw, axis=-1, keepdims=True) + norm_epsilon)
         base = (raw * root * latent_gain_ref[...]).astype(narrow)
         turned_keys = turned(rotary_values, where).T.astype(narrow)
@@ -435,17 +447,21 @@
             state[group + 2 : group + 3] = amount
             numerator[spots, :] = mixed
 
-    fold(0, rotary_ref[...], own_places, True, True)
+    fold(0, slice(None), rotary_ref[...], own_places, True, True)
 
     @pl.when(sp == 1)
     def _():
-        there = latents.at[1, mine, :]
-        settle(there, cross_sem.at[0])
-        passed = push(there, there, cross_back.at[0], cross_sem.at[3], core_device)
         settle(rotaries, cross_sem.at[1])
-        passed.wait_recv()
-        fold(1, rotaries[...], pl.ds(0, seq_rows), False, False)
-        passed.wait_send()
+        for number in range(PIECES):
+            here = piece(core, number)
+            there = latents.at[1, here, :]
+            settle(there, cross_sem.at[3 + number])
+            push(there, there, cross_back.at[0], cross_sem.at[3 + PIECES + number], core_device)
+            fold(1, here, rotaries[:, here], here, False, False)
+            here = piece(1 - core, number)
+            settle(latents.at[1, here, :], cross_sem.at[3 + PIECES + number])
+            fold(1, here, rotaries[:, here], here, False, False)
+        settle(latents.at[1, mine, :], cross_back.at[0])
 
     @pl.when(sp == 0)
     def _():
@@ -500,7 +516,7 @@
         part[chunk, :, row, core] = (
             part[chunk, :, row, core].astype(wide) + side_land[chunk].astype(wide)
         ).astype(narrow)
-        for m in range(1, lines):
+        for m in range(lines - 1, 0, -1):
             push(
                 part.at[chunk, at_line[m], row, core],
                 line_land.at[chunk, m - 1],
@@ -518,13 +534,9 @@
         middle_ref[:, columns] = (residual[:, columns].astype(wide) + value).astype(narrow)
 
     stages = (to_side, to_line, close)
-    for step in range(chunks + len(stages)):
-        if step < chunks:
-            project(step)
-        for number, stage in enumerate(stages):
-            chunk = step - 1 - number
-            if 0 <= chunk < chunks:
-                stage(chunk)
+    for stage in (project, *stages):
+        for chunk in range(chunks):
+            stage(chunk)
     middle = middle_ref[...].astype(wide)
     root = lax.rsqrt(jnp.mean(middle * middle, axis=-1, keepdims=True) + norm_epsilon)
     normed_ref[...] = (middle * root * expert_gain_ref[...]).astype(narrow)
@@ -621,7 +633,7 @@
     def send_own(chunk):
         source = x_ref.at[:, pl.ds(chunk * width, width)]
         target = tok.at[chunk, sp, line, row, core]
-        for m in range(1, lines):
+        for m in range(lines - 1, 0, -1):
             push(source, target, pass_sem.at[chunk, 2], line_sem.at[chunk, m - 1], line_device[m])
         push(source, target, pass_sem.at[chunk, 0], side_sem.at[chunk, 0, 0], x_device)
         push(source, target, pass_sem.at[chunk, 0], side_sem.at[chunk, 1, 0], y_device)
@@ -667,7 +679,7 @@
         for number in range(4):
             settle(tok.at[chunk, 0, :, 0, 0], core_sem.at[chunk, number])
 
-    for chunk in range(chunks):
+    for chunk in range(EARLY):
         send_own(chunk)
     for chunk in range(chunks):
         tok[chunk, sp, line, row, core] = x_ref[:, chunk * width : (chunk + 1) * width]
@@ -720,27 +732,12 @@
 
         lax.fori_loop(low, high, one, 0, unroll=2)
 
-    clock = [0]
-
-    def tick():
-        now = clock[0]
-        clock[0] = now + 1
-        for stage, lag in ((pass_line, 0), (pass_side, LAGS[0]), (pass_diag, LAGS[1])):
-            if 0 <= now - lag < chunks:
-                stage(now - lag)
-
-    def reach(chunk):
-        while clock[0] <= min(chunk + LAGS[2], chunks - 1) + LAGS[1]:
-            tick()
-
-    for step in range(steps):
-        for number in range(joined):
-            reach(step * joined + number)
-            pick(step * joined + number)
+    def first_half(step):
         for copy in weight_copies(step):
             copy.wait()
         hidden(step, 0, experts // 2)
-        reach((step + 1) * joined)
+
+    def second_half(step):
         hidden(step, experts // 2, experts)
         if step + 2 < steps:
             for copy in weight_copies(step + 2):
@@ -748,6 +745,18 @@
         if step == 0:
             for later in range(chunks):
                 down_copy(later).start()
+
+    moves = {
+        "O": send_own,
+        "L": pass_line,
+        "S": pass_side,
+        "D": pass_diag,
+        "P": pick,
+        "A": first_half,
+        "B": second_half,
+    }
+    for move in ORDER:
+        moves[move[0]](int(move[1:]))
 
     for chunk in range(chunks):
         settle(core_land.at[chunk, 0], pass_sem.at[chunk, 0])
@@ -846,7 +855,7 @@
             row,
             side_land[chunk, 0].astype(jnp.float32) + side_land[chunk, 1].astype(jnp.float32),
         )
-        for m in range(1, lines):
+        for m in range(lines - 1, 0, -1):
             push(
                 tok.at[chunk, sp, at_line[m], row, core],
                 line_land.at[chunk, m - 1],
@@ -1010,7 +1019,7 @@
         keep((STRIPS, lines, rows, strip), narrow),
         keep((STRIPS, lines - 1, rows, strip), narrow),
         keep((STRIPS, rows, strip), wide),
-        dma((4,)),
+        dma((3 + 2 * PIECES,)),
         dma((3,)),
         dma((STRIPS,)),
         dma((STRIPS,)),

time: 102 us -> 100 us (0.980)
  Pallas kernels: 100 us -> 98.6 us
    pallas_call x1, Pallas kernels: 100 us -> 98.6 us  [run_layer(): pl.pallas_call(functools.partial(layer_kernel, pitch, names, len(attentio...]
where the time goes in v4:
time: 100 us
  Pallas kernels  98.6 us (99%)
  other arithmetic  1.66 us (2%)
    pallas_call x1, Pallas kernels, run_layer(): pl.pallas_call(functools.partial(layer_kernel, pitch, names, len(attentio...  98.6 us

profile of v4, /device:TPU:0, one launch (start us, length us, event | category | flops | bytes accessed | tf_op | source)
XLA Modules:
  0.0 100.3 jit_solution(15968546576661608265)
XLA Ops:
  0.0 98.6 %run_layer.1 = (f32[32,2048]{1,0:T(8,128)}, bf16[32,2048]{1,0:T(8,128)(2,1)}) custom-call(f32[32,1024]{1,0:T(8,128)} %constant.2.clone.refs_0_, bf16[96,512]{1,0:T(8,128)(2,1)} %bitcast.10, bf16[160,512]{1,0:T(8,128)(2,1)} %bitcast.9, bf16[32,512]{1,0:T(8,128)(2,1)} %bitcast.13, f32[1,512]{1,0:T(1,128)} %bitcast.17, bf16[64,512]{1,0:T(8,128)(2,1)} %bitcast.11, ...), custom_call_target="tpu_custom_call" | custom-call | tf_op jit(solution)/shard_map/run_layer/pallas_call | solution.py:1069
  98.6 1.7 %add_convert_fusion = bf16[32,2048]{1,0:T(8,128)(2,1)} fusion(f32[32,2048]{1,0:T(8,128)} %get-tuple-element.8, bf16[32,2048]{1,0:T(8,128)(2,1)} %get-tuple-element.7), kind=kLoop, calls=%fused_computation | loop fusion | flops 196608 | bytes 524288 | tf_op jit(solution)/shard_map/convert_element_type | solution.py:1136
